TPU v7x, 256 devices: a whole 4x4x8 slice. The times are simulated.
256 devices in a mesh: ep: 128 (over z, y, x), tp: 2 (over core).
Axes of the slice: x: 4, y: 4, z: 8, core: 2. Of those that a mesh axis runs over, the one named last changes fastest.
Arguments:
- tokens: bfloat16 [4096, 1024], P('ep'), may hold values from -6 to 6
- norm_gain: float32 [1024], replicated, may hold values from 0.1 to 1.9
- routing: int32 [4096, 4], P('ep'), may hold values from 0 to 127, all different within a row; in each aligned block of 32 rows (0 to 31, 32 to 63, ...) at most 16 rows name the same one
- route_logits: float32 [4096, 4], P('ep'), may hold values from -6 to 6
- w_gate: bfloat16 [128, 1024, 1024], P('ep', None, 'tp'), may hold values from -0.1875 to 0.1875
- w_up: bfloat16 [128, 1024, 1024], P('ep', None, 'tp'), may hold values from -0.1875 to 0.1875
- w_down: bfloat16 [128, 1024, 1024], P('ep', None, 'tp'), may hold values from -0.1875 to 0.1875
Outputs:
- mixed: bfloat16 [4096, 1024], P('ep', 'tp')
Inputs may be any that keep to these rules, and one draw needn't show every extreme that they name: `routing`: each row names 4 different experts; among the 32 tokens of one index of ep (aligned blocks of rows) no expert is named by more than 16 rows, and some block has an expert named by exactly 16.
All inputs are finite; a program needn't handle non-finite values.
Results may differ from a plain program's by a relative error of at most 0.0085.
Values may be sent and summed in bfloat16 or wider, within the bound.
A program may use at most 64 MiB of HBM per device.

v0:
```python
import jax
import jax.numpy as jnp
from jax import lax
from jax.sharding import PartitionSpec as P

CAP = 16


eps = 1e-05


def taken_in(share, axis, dim, step, start):
    def gathered(part):
        return lax.all_gather(part, axis, axis=dim, tiled=True)

    return step(start, jax.tree.map(gathered, share), jnp.int32(0))


def clamped(gate_part, up_part):
    limited = jnp.minimum(gate_part, 7.0)
    linear = jnp.clip(up_part, -7.0, 7.0)
    return limited * jax.nn.sigmoid(1.702 * limited) * (linear + 1.0)


def expert_rows(rows, w_gate, w_up, w_down):
    gate_part = jnp.dot(rows, w_gate[0], preferred_element_type=jnp.float32)
    up_part = jnp.dot(rows, w_up[0], preferred_element_type=jnp.float32)
    hidden = clamped(gate_part, up_part).astype(jnp.bfloat16)
    down_local = w_down[0]
    empty = jnp.zeros((rows.shape[0], down_local.shape[1]), jnp.float32)

    def add_rows(total, piece, start):
        weights = lax.dynamic_slice_in_dim(down_local, start, piece.shape[1], 0)
        return total + jnp.dot(piece, weights, preferred_element_type=jnp.float32)

    summed = taken_in(hidden, "tp", 1, add_rows, empty)
    return summed.astype(jnp.bfloat16)


def shards(tokens, norm_gain, routing, route_logits, w_gate, w_up, w_down):
    as_float = tokens.astype(jnp.float32)
    scaled = as_float * lax.rsqrt(jnp.mean(as_float * as_float, axis=-1, keepdims=True) + eps)
    normed = (scaled * norm_gain).astype(jnp.bfloat16)
    gate_probs = jax.nn.softmax(route_logits, axis=-1)
    tok_dev = tokens.shape[0]
    topk = routing.shape[1]
    width = tokens.shape[1]
    n_ep = lax.axis_size("ep")
    assigns = tok_dev * topk
    flat_e = routing.reshape(-1)
    onehot = (flat_e[:, None] == jnp.arange(n_ep, dtype=jnp.int32)[None, :]).astype(jnp.int32)
    slot_rank = jnp.sum((jnp.cumsum(onehot, axis=0) - onehot) * onehot, axis=1).astype(jnp.int32)
    slot_index = flat_e * CAP + slot_rank
    flat_tok = jnp.arange(assigns, dtype=jnp.int32) // topk
    outbound = jnp.zeros((n_ep * CAP, width), jnp.bfloat16).at[slot_index].set(normed[flat_tok])
    arrived = lax.all_to_all(
        outbound.reshape(n_ep, CAP, width), "ep", split_axis=0, concat_axis=0, tiled=True
    )
    expert_out = expert_rows(arrived.reshape(n_ep * CAP, width), w_gate, w_up, w_down)
    half_width = expert_out.shape[1]
    returned_rows = lax.all_to_all(
        expert_out.reshape(n_ep, CAP, half_width), "ep", split_axis=0, concat_axis=0, tiled=True
    )
    returned_rows = returned_rows.reshape(n_ep * CAP, half_width)
    picked = returned_rows[slot_index].astype(jnp.float32) * gate_probs.reshape(-1)[:, None]
    mixed = jnp.sum(picked.reshape(tok_dev, topk, half_width), axis=1).astype(jnp.bfloat16)
    return mixed


def solution(mesh):
    return jax.shard_map(
        shards,
        mesh=mesh,
        in_specs=(
            P("ep", None),
            P(),
            P("ep", None),
            P("ep", None),
            P("ep", None, "tp"),
            P("ep", None, "tp"),
            P("ep", None, "tp"),
        ),
        out_specs=P("ep", "tp"),
        check_vma=False,
    )
```

profile of v0, /device:TPU:1, one launch (start us, length us, event | category | flops | bytes accessed | tf_op | source)
XLA Modules:
  0.0 233.8 jit_solution(14845142519807675940)
XLA Ops:
  6.5 0.8 copy.12
  7.4 0.7 broadcast_multiply_fusion
  8.1 0.1 eq.15
  8.2 0.1 fusion.10
  8.3 0.2 reduce_window_sum.11
  8.5 0.2 select_reduce_fusion
  8.6 0.1 copy.11
  8.7 0.1 mul.61
  8.8 1.0 fusion.7
  9.8 0.9 fusion.9
  10.8 4.8 %scatter_custom_fusion = bf16[2048,1024]{1,0:T(8,128)(2,1)} fusion(s32[128]{0:T(128)S(1)} %fusion.14, bf16[]{:T(256)} %constant.17.clone.1, bf16[32,1024]{1,0:T(8,128)(2,1)S(1)} %fusion.9, s32[1024]{0:T(1024)S(1)} %pad_clamp_fusion.1), kind=kCustom, calls=%fused_computation.5 | custom fusion | bytes 4194306 | tf_op jit(solution)/shard_map/scatter | solution.py:55
  15.5 111.8 %all_to_all.10 = bf16[128,16,1024]{2,1,0:T(8,128)(2,1)S(1)} all-to-all(bf16[128,16,1024]{2,1,0:T(8,128)(2,1)} %bitcast.24), channel_id=1, replica_groups=mesh['ep'=128,'tp'=2] {'ep'}, dimensions={0} | all-to-all | bytes 8388608 | tf_op jit(solution)/shard_map/all_to_all | solution.py:56
  127.3 2.3 %fusion.4 = f32[2048,512]{1,0:T(8,128)S(1)} fusion(bf16[2048,1024]{1,0:T(8,128)(2,1)S(1)} %bitcast.26, bf16[1,1024,512]{2,1,0:T(8,128)(2,1)S(1)} %copy-done), kind=kOutput, calls=%fused_computation.9 | convolution fusion | flops 2147483648 | bytes 9437184 | tf_op jit(solution)/shard_map/dot_general | solution.py:26
  129.7 0.0 copy-start.3
  129.7 4.8 %multiply_convert_fusion = bf16[2048,512]{1,0:T(8,128)(2,1)} fusion(f32[2048,512]{1,0:T(8,128)S(1)} %fusion.4, bf16[2048,1024]{1,0:T(8,128)(2,1)S(1)} %bitcast.27, bf16[1,1024,512]{2,1,0:T(8,128)(2,1)S(1)} %copy-done.2), kind=kOutput, calls=%fused_computation.3 | convolution fusion | flops 2157969408 | bytes 11534336 | tf_op jit(solution)/shard_map/dot_general | solution.py:27
  134.6 0.0 all-gather.2.cloned.1.call-update
  134.6 18.6 %all-gather.2.cloned.1.call-done = bf16[2048,1024]{1,0:T(8,128)(2,1)} async-done(((bf16[2048,512]{1,0:T(8,128)(2,1)}), bf16[2048,1024]{1,0:T(8,128)(2,1)}) %all-gather.2.cloned.1.call-update) | async-done | bytes 4194320 | tf_op jit(solution)/shard_map/all_gather | solution.py:14
  153.2 5.9 %convolution_convert_fusion = bf16[2048,512]{1,0:T(8,128)(2,1)} fusion(bf16[2048,1024]{1,0:T(8,128)(2,1)} %all-gather.2.cloned.1.call-done, bf16[1,1024,512]{2,1,0:T(8,128)(2,1)S(1)} %copy-done.3), kind=kOutput, calls=%fused_computation.4 | convolution fusion | flops 2148532224 | bytes 7340032 | tf_op jit(solution)/shard_map/dot_general | solution.py:34
  159.1 13.7 %all-to-all-start.1 = ((bf16[128,16,512]{2,1,0:T(8,128)(2,1)}), bf16[128,16,512]{2,1,0:T(8,128)(2,1)S(1)}, u32[]{:S(2)}, u32[]{:S(2)}) async-start(bf16[128,16,512]{2,1,0:T(8,128)(2,1)} %bitcast.28), calls=%async_computation.1 | async-start | bytes 4194304 | tf_op jit(solution)/shard_map/all_to_all | solution.py:61
  172.8 0.1 copy.13
  172.9 52.2 %all-to-all-done.1 = bf16[128,16,512]{2,1,0:T(8,128)(2,1)S(1)} async-done(((bf16[128,16,512]{2,1,0:T(8,128)(2,1)}), bf16[128,16,512]{2,1,0:T(8,128)(2,1)S(1)}, u32[]{:S(2)}, u32[]{:S(2)}) %all-to-all-start.1) | async-done | bytes 2097184 | tf_op jit(solution)/shard_map/all_to_all | solution.py:61
  225.1 0.8 gather_fusion
  226.0 0.1 reshape.110
  226.1 0.8 multiply_reduce_fusion
  (16 shorter events, 0.1 us)
Async XLA Ops:
  6.5 120.8 %copy-start = (bf16[1,1024,512]{2,1,0:T(8,128)(2,1)S(1)}, bf16[1,1024,512]{2,1,0:T(8,128)(2,1)}, u32[]{:S(2)}) copy-start(bf16[1,1024,512]{2,1,0:T(8,128)(2,1)} %param.11) | copy-start | bytes 3145732
  6.5 146.6 %all-gather.2.cloned.1.call-start = ((), (), s32[]{:S(2)}) async-start(), calls=%async_computation.2 | async-start | bytes 6291456 | tf_op jit(solution)/shard_map/all_gather | solution.py:14
  127.3 2.3 %copy-start.2 = (bf16[1,1024,512]{2,1,0:T(8,128)(2,1)S(1)}, bf16[1,1024,512]{2,1,0:T(8,128)(2,1)}, u32[]{:S(2)}) copy-start(bf16[1,1024,512]{2,1,0:T(8,128)(2,1)} %param.12) | copy-start | bytes 3145732
  129.7 23.5 %copy-start.3 = (bf16[1,1024,512]{2,1,0:T(8,128)(2,1)S(1)}, bf16[1,1024,512]{2,1,0:T(8,128)(2,1)}, u32[]{:S(2)}) copy-start(bf16[1,1024,512]{2,1,0:T(8,128)(2,1)} %param.13) | copy-start | bytes 3145732
  159.1 13.7 %copy-start.1 = (f32[32,4]{0,1:T(4,128)S(1)}, f32[32,4]{0,1:T(4,128)}, u32[]{:S(2)}) copy-start(f32[32,4]{0,1:T(4,128)} %param.10) | copy-start | bytes 1540
  159.1 66.1 %all-to-all-start.1 = ((bf16[128,16,512]{2,1,0:T(8,128)(2,1)}), bf16[128,16,512]{2,1,0:T(8,128)(2,1)S(1)}, u32[]{:S(2)}, u32[]{:S(2)}) async-start(bf16[128,16,512]{2,1,0:T(8,128)(2,1)} %bitcast.28), calls=%async_computation.1 | async-start | bytes 4194304 | tf_op jit(solution)/shard_map/all_to_all | solution.py:61
Sparse Core Ops, SparseCore 0:
  134.7 18.4 all-gather.1
where the time goes:
time: 234 us
  blocking collectives  112 us (48%)
  waiting for transfers between devices  70.8 us (30%)
  starting transfers between devices  13.7 us (6%)
  between operations  13.5 us (6%)
  matrix products  13.1 us (6%)
  local copies, waits for them, and re-layouts  6.95 us (3%)
  other arithmetic  3.94 us (2%)
    all_to_all x1, blocking collectives, shards(): lax.all_to_all(outbound.reshape(n_ep, CAP, width), 'ep', split_axis=0, co...  112 us
    all_to_all x1, waiting for transfers between devices, shards(): lax.all_to_all(expert_out.reshape(n_ep, CAP, half_width), 'ep', split_axi...  52.2 us
    all_gather x1, waiting for transfers between devices, gathered(): return lax.all_gather(part, axis, axis=dim, tiled=True)  18.6 us
    all_to_all x1, starting transfers between devices, shards(): lax.all_to_all(expert_out.reshape(n_ep, CAP, half_width), 'ep', split_axi...  13.7 us
    dot_general x1, matrix products, add_rows(): return total + jnp.dot(piece, weights, preferred_element_type=jnp.float32)  5.87 us
    dot_general x1, matrix products, expert_rows(): up_part = jnp.dot(rows, w_up[0], preferred_element_type=jnp.float32)  4.84 us
    scatter x1, local copies, waits for them, and re-layouts, shards(): jnp.zeros((n_ep * CAP, width), jnp.bfloat16).at[slot_index]  4.75 us
  transfers between devices with their start and end apart: 2, of which 2 were waited for; matrix products, arithmetic and copies ran while one was open for 0% of the time, Pallas kernels for 0%

commit v1 on v0

v1 whole, which is shorter than its diff:
```python
import jax
import jax.numpy as jnp
from jax import lax
from jax.sharding import PartitionSpec as P

eps = 1e-05


def clamped(gate_part, up_part):
    limited = jnp.minimum(gate_part, 7.0)
    linear = jnp.clip(up_part, -7.0, 7.0)
    return limited * jax.nn.sigmoid(1.702 * limited) * (linear + 1.0)


def shards(tokens, norm_gain, routing, route_logits, w_gate, w_up, w_down):
    as_float = tokens.astype(jnp.float32)
    scaled = as_float * lax.rsqrt(jnp.mean(as_float * as_float, axis=-1, keepdims=True) + eps)
    normed = (scaled * norm_gain).astype(jnp.bfloat16)
    probs = jax.nn.softmax(route_logits, axis=-1)
    half = normed.shape[1] // 2
    mine = lax.dynamic_slice_in_dim(normed, lax.axis_index("tp") * half, half, 1)
    n_ep = lax.axis_size("ep")
    expert = lax.axis_index("ep")
    onehot = routing[:, :, None] == jnp.arange(n_ep, dtype=jnp.int32)
    weights = jnp.sum(jnp.where(onehot, probs[:, :, None], 0.0), axis=1)
    arrived_w = lax.all_to_all(weights.T, "ep", split_axis=0, concat_axis=0, tiled=True)
    rows = lax.all_gather(mine, "ep", axis=0, tiled=True)
    rows = lax.all_gather(rows, "tp", axis=1, tiled=True)
    gate_part = jnp.dot(rows, w_gate[0], preferred_element_type=jnp.float32)
    up_part = jnp.dot(rows, w_up[0], preferred_element_type=jnp.float32)
    hidden = clamped(gate_part, up_part).astype(jnp.bfloat16)
    hidden = lax.all_gather(hidden, "tp", axis=1, tiled=True)
    out = jnp.dot(hidden, w_down[0], preferred_element_type=jnp.float32)
    out = out * arrived_w.reshape(-1, 1)
    return lax.psum_scatter(out.astype(jnp.bfloat16), "ep", scatter_dimension=0, tiled=True)


def solution(mesh):
    return jax.shard_map(
        shards,
        mesh=mesh,
        in_specs=(
            P("ep", None),
            P(),
            P("ep", None),
            P("ep", None),
            P("ep", None, "tp"),
            P("ep", None, "tp"),
            P("ep", None, "tp"),
        ),
        out_specs=P("ep", "tp"),
        check_vma=False,
    )
```

time: 234 us -> 924 us (3.95)
  the two profiles are of different devices: /device:TPU:1 before, /device:TPU:0 now
where the time goes in v1:
time: 924 us
  waiting for transfers between devices  853 us (92%)
  blocking collectives  27 us (3%)
  matrix products  25.8 us (3%)
  between operations  13.2 us (1%)
    reduce_scatter x1, waiting for transfers between devices, shards(): lax.psum_scatter(out.astype(jnp.bfloat16), 'ep', scatter_dimension=0, til...  709 us
    all_gather x1, waiting for transfers between devices, shards(): rows = lax.all_gather(mine, 'ep', axis=0, tiled=True)  119 us
    all_to_all x1, blocking collectives, shards(): lax.all_to_all(weights.T, 'ep', split_axis=0, concat_axis=0, tiled=True)  27 us
    all_gather x1, waiting for transfers between devices, shards(): rows = lax.all_gather(rows, 'tp', axis=1, tiled=True)  24.1 us
  transfers between devices with their start and end apart: 4, of which 3 were waited for; matrix products, arithmetic and copies ran while one was open for 0% of the time, Pallas kernels for 0%

profile of v1, /device:TPU:0, one launch (start us, length us, event | category | flops | bytes accessed | tf_op | source)
XLA Modules:
  0.0 923.9 jit_solution(12869763344411301815)
XLA Ops:
  6.5 0.9 convert_element_type.12
  7.5 1.0 multiply_reduce_fusion
  8.5 0.8 dynamic-slice
  9.2 0.7 fusion.5
  9.9 0.0 all-gather.4.cloned.1.call-update
  9.9 0.0 all-gather.6.cloned.1.call-start
  10.0 119.2 %all-gather.4.cloned.1.call-done = bf16[4096,512]{1,0:T(8,128)(2,1)} async-done(((bf16[32,512]{1,0:T(8,128)(2,1)}), bf16[4096,512]{1,0:T(8,128)(2,1)}) %all-gather.4.cloned.1.call-update) | async-done | bytes 4194320 | tf_op jit(solution)/shard_map/all_gather | solution.py:27
  129.2 0.0 all-gather.6.cloned.1.call-update
  129.3 0.0 all-gather.8.cloned.1.call-start
  129.3 24.1 %all-gather.6.cloned.1.call-done = bf16[4096,1024]{1,0:T(8,128)(2,1)} async-done(((bf16[4096,512]{1,0:T(8,128)(2,1)}), bf16[4096,1024]{1,0:T(8,128)(2,1)}) %all-gather.6.cloned.1.call-update) | async-done | bytes 8388624 | tf_op jit(solution)/shard_map/all_gather | solution.py:28
  153.4 7.7 fusion.1
  161.2 8.6 multiply_convert_fusion.1
  169.9 0.0 all-gather.8.cloned.1.call-update
  169.9 0.0 reduce-scatter.2.cloned.1.call-start
  170.0 0.1 select_reduce_fusion
  170.1 0.1 copy.14
  170.2 27.0 %all_to_all.9 = f32[128,1,32]{2,1,0:T(1,128)S(1)} all-to-all(f32[128,1,32]{2,1,0:T(1,128)S(1)} %copy.14), channel_id=1, replica_groups=mesh['ep'=128,'tp'=2] {'ep'}, dimensions={0} | all-to-all | bytes 32768 | tf_op jit(solution)/shard_map/all_to_all | solution.py:26
  197.2 0.5 broadcast.24
  197.7 0.8 reduce.3
  198.5 0.1 mul.54
  198.6 0.0 all-gather.8.cloned.1.call-done
  198.6 9.5 %multiply_convert_fusion = bf16[4096,512]{1,0:T(8,128)(2,1)} fusion(bf16[4096,1024]{1,0:T(8,128)(2,1)} %all-gather.8.cloned.1.call-done, f32[4096]{0:T(1024)S(1)} %mul.54, bf16[1,1024,512]{2,1,0:T(8,128)(2,1)S(1)} %copy-done.5), kind=kOutput, calls=%fused_computation | convolution fusion | flops 4299161600 | bytes 13647872 | tf_op jit(solution)/shard_map/dot_general | solution.py:33
  208.1 0.0 reduce-scatter.2.cloned.1.call-update
  208.1 709.3 %reduce-scatter.2.cloned.1.call-done = bf16[32,512]{1,0:T(8,128)(2,1)} async-done(((bf16[4096,512]{1,0:T(8,128)(2,1)}), bf16[32,512]{1,0:T(8,128)(2,1)}) %reduce-scatter.2.cloned.1.call-update) | async-done | bytes 32784 | tf_op jit(solution)/shard_map/reduce_scatter | solution.py:35
  (17 shorter events, 0.1 us)
Async XLA Ops:
  6.5 146.9 %copy-start = (bf16[1,1024,512]{2,1,0:T(8,128)(2,1)S(1)}, bf16[1,1024,512]{2,1,0:T(8,128)(2,1)}, u32[]{:S(2)}) copy-start(bf16[1,1024,512]{2,1,0:T(8,128)(2,1)} %param.12) | copy-start | bytes 3145732
  6.5 122.7 %all-gather.4.cloned.1.call-start = ((), (), s32[]{:S(2)}) async-start(), calls=%async_computation.2 | async-start | bytes 4227072 | tf_op jit(solution)/shard_map/all_gather | solution.py:27
  9.9 143.5 %all-gather.6.cloned.1.call-start = ((), (), s32[]{:S(2)}) async-start(), calls=%async_computation.3 | async-start | bytes 12582912 | tf_op jit(solution)/shard_map/all_gather | solution.py:28
  129.3 31.9 %copy-start.4 = (bf16[1,1024,512]{2,1,0:T(8,128)(2,1)S(1)}, bf16[1,1024,512]{2,1,0:T(8,128)(2,1)}, u32[]{:S(2)}) copy-start(bf16[1,1024,512]{2,1,0:T(8,128)(2,1)} %param.11) | copy-start | bytes 3145732
  129.3 69.3 %all-gather.8.cloned.1.call-start = ((), (), s32[]{:S(2)}) async-start(), calls=%async_computation.4 | async-start | bytes 12582912 | tf_op jit(solution)/shard_map/all_gather | solution.py:32
  153.4 7.8 copy-start.3
  161.2 8.7 copy-start.1
  161.2 8.8 copy-start.2
  161.2 37.4 %copy-start.5 = (bf16[1,1024,512]{2,1,0:T(8,128)(2,1)S(1)}, bf16[1,1024,512]{2,1,0:T(8,128)(2,1)}, u32[]{:S(2)}) copy-start(bf16[1,1024,512]{2,1,0:T(8,128)(2,1)} %param.13) | copy-start | bytes 3145732
  169.9 747.5 %reduce-scatter.2.cloned.1.call-start = ((), (), s32[]{:S(2)}) async-start(), calls=%async_computation.5 | async-start | bytes 4227072 | tf_op jit(solution)/shard_map/reduce_scatter | solution.py:35
Sparse Core Ops, SparseCore 0:
  10.9 118.2 all-gather.3
  131.0 22.3 all-gather.5
  170.0 26.4 all-gather.7
  208.2 709.0 reduce-scatter.1

commit v2 on v1

v2 whole, which is shorter than its diff:
```python
import jax
import jax.numpy as jnp
from jax import lax
from jax.experimental import pallas as pl
from jax.experimental.pallas import tpu as pltpu
from jax.sharding import PartitionSpec as P

MESH = pl.DeviceIdType.MESH
NX, NY, NZ = 4, 4, 8
CAP = 16
BLK = 32
HALF = 256
ROWS = BLK + 8
EPS = 1e-05
BF = jnp.bfloat16
F32 = jnp.float32
ARRIVAL = (0, 1, 7, 2, 6, 3, 5, 4)


def iota(shape, dim):
    return lax.broadcasted_iota(jnp.int32, shape, dim)


def kernel(
    tok_hbm, gain_hbm, ids_hbm, log_hbm, wg_hbm, wu_hbm, wd_hbm, out_ref,
    tok, gain, ids, logits, wg, wu, wd,
    own, ybuf, sbuf, xown, xoth, hown, hoth, ysend, r1buf, pacc, r2send, r2buf, r3send, r3buf,
    in_sem, w_sem, z_send, z_recv, s2_send, s2_recv, s3_send, s3_recv, x_send, x_recv,
    h_send, h_recv, r1_send, r1_recv, r2_send, r2_recv, r3_send, r3_recv,
):
    ep = lax.axis_index("ep")
    c = lax.axis_index("tp")
    x = lax.rem(ep, NX)
    y = lax.rem(ep // NX, NY)
    z = ep // (NX * NY)

    def at(dx=0, dy=0, dz=0):
        px = lax.rem(x + dx, NX)
        py = lax.rem(y + dy, NY)
        pz = lax.rem(z + dz, NZ)
        return ((pz * NY + py) * NX + px, c)

    partner = (ep, 1 - c)

    def peer(col, j):
        return at(dy=j) if col == 0 else at(dx=j)

    def far(col, j):
        return at(dx=j) if col == 0 else at(dy=j)

    def remote(src, dst, send, recv, device):
        return pltpu.make_async_remote_copy(
            src_ref=src, dst_ref=dst, send_sem=send, recv_sem=recv, device_id=device, device_id_type=MESH
        )

    def drain(ref, sem):
        pltpu.make_async_copy(ref, ref, sem).wait()

    small = [
        pltpu.make_async_copy(tok_hbm, tok, in_sem.at[0]),
        pltpu.make_async_copy(gain_hbm, gain, in_sem.at[1]),
        pltpu.make_async_copy(ids_hbm, ids, in_sem.at[2]),
        pltpu.make_async_copy(log_hbm, logits, in_sem.at[3]),
    ]
    for copy in small:
        copy.start()
    weights = []
    for i, (src, dst) in enumerate(((wg_hbm, wg), (wu_hbm, wu), (wd_hbm, wd))):
        for part in range(2):
            start = pl.multiple_of(lax.rem(c + part, 2) * 512, 512)
            weights.append(
                pltpu.make_async_copy(src.at[pl.ds(start, 512)], dst.at[pl.ds(part * 512, 512)], w_sem.at[i, part])
            )
    for copy in weights:
        copy.start()

    barrier = pltpu.get_barrier_semaphore()
    friends = [at(dz=k) for k in range(1, NZ)] + [at(dy=j) for j in range(1, NY)] + [at(dx=j) for j in range(1, NX)]
    friends.append(partner)
    for friend in friends:
        pl.semaphore_signal(barrier, inc=1, device_id=friend, device_id_type=MESH)

    for copy in small:
        copy.wait()

    full = tok[...].astype(F32)
    scale = lax.rsqrt(jnp.mean(full * full, axis=-1, keepdims=True) + EPS)
    mine = pl.ds(pl.multiple_of(c * 512, 512), 512)
    normed = (tok[:, mine].astype(F32) * scale * gain[:, mine]).astype(BF)

    lane4 = iota((BLK, 128), 1)
    spread = (lax.rem(lane4, BLK) == iota((BLK, 128), 0)).astype(BF)
    raw = logits[...]
    shifted = jnp.exp(raw - jnp.max(raw, axis=0, keepdims=True))
    probs = shifted / jnp.sum(shifted, axis=0, keepdims=True)
    ids_l = jnp.dot(ids[...].astype(F32).astype(BF), spread, preferred_element_type=F32)
    probs_l = jnp.dot(probs.astype(BF), spread, preferred_element_type=F32)
    row = iota((128, 128), 0)
    lane = iota((128, 128), 1)
    plane = lax.rem(z + row // 16, NZ)
    near = lax.rem(row, 4)
    group = lane // BLK
    route_b = lax.rem(row // 8, 2) == 0
    ex = lax.rem(x + jnp.where(route_b, near, group), NX)
    ey = lax.rem(y + jnp.where(route_b, group, near), NY)
    expert = (plane * 16 + ey * NX + ex).astype(F32)
    named = jnp.zeros((128, 128), F32)
    weight = jnp.zeros((128, 128), F32)
    for q in range(4):
        hit = expert == ids_l[q : q + 1, :]
        named = jnp.where(hit, 1.0, named)
        weight = jnp.where(hit, probs_l[q : q + 1, :], weight)
    before = ((row // BLK == lane // BLK) & (row < lane)).astype(BF)
    place = jnp.dot(named.astype(BF), before, preferred_element_type=F32)
    place = jnp.where(named > 0, place, -128.0)
    meta = jnp.where(lax.rem(row, 8) < 4, place, weight).astype(BF)
    blank = jnp.zeros((8, HALF - 128), BF)
    for k in range(NZ):
        for col in range(2):
            dst = own.at[k, col] if k else ybuf.at[0, col, 0]
            dst[:BLK, :] = normed[:, col * HALF : (col + 1) * HALF]
            dst[BLK:, :128] = meta[k * 16 + col * 8 : k * 16 + col * 8 + 8, :]
            dst[BLK:, 128:] = blank

    pl.semaphore_wait(barrier, len(friends))

    def start_z():
        for k in (1, 7, 2, 6, 3, 5, 4):
            slot = (-k) % NZ
            remote(own.at[k], ybuf.at[slot, :, 0], z_send, z_recv.at[slot], at(dz=k)).start()

    def s2(k):
        if k:
            drain(own.at[k], z_recv.at[k])
        for j in (1, 3, 2):
            for col in range(2):
                remote(
                    ybuf.at[k, col, 0], ybuf.at[k, col, (-j) % 4], s2_send, s2_recv.at[k, col], peer(col, j)
                ).start()

    lanes = iota((8, 128), 1) // BLK
    sixty = iota((64, 128), 0)
    base = (iota((1, 128), 1) // BLK * CAP).astype(F32)

    def table(k, col):
        t = [ybuf[k, col, s, BLK:, :128].astype(F32) for s in range(4)]
        t1 = pltpu.roll(t[1], 64, 1)
        t3 = pltpu.roll(t[3], 64, 1)
        return jnp.where(lanes == 0, t[0], jnp.where(lanes == 1, t1, jnp.where(lanes == 2, t[2], t3)))

    def select(k, col, weighted):
        m = table(k, col)
        parts = []
        for j in range(4):
            wanted = (m[j : j + 1, :] + base).astype(jnp.int32)
            value = m[4 + j : 5 + j, :] if weighted else 1.0
            parts.append(jnp.where(sixty == wanted, value, 0.0).astype(BF))
        return jnp.concatenate(parts, axis=0)

    def s3(k):
        for col in range(2):
            drain(ybuf.at[k, col, pl.ds(1, 3)], s2_recv.at[k, col])
            rows = ybuf[k, col, :, :BLK, :].reshape(128, HALF)
            packed = jnp.dot(select(k, col, False), rows, preferred_element_type=F32).astype(BF)
            for j in range(4):
                piece = packed[64 * j : 64 * j + 64].reshape(4, CAP, HALF)
                if j:
                    sbuf[k, col, j - 1] = piece
                elif col == 0:
                    xown[k, 0, 0] = piece
                else:
                    xown[k, 1, :, 0] = piece
            for j in (1, 3, 2):
                slot = (-j) % 4
                dst = xown.at[k, 0, slot] if col == 0 else xown.at[k, 1, :, slot]
                remote(sbuf.at[k, col, j - 1], dst, s3_send, s3_recv.at[k, col], far(col, j)).start()

    def x4(k):
        for col in range(2):
            drain(sbuf.at[k, col], s3_recv.at[k, col])
        remote(xown.at[k], xoth.at[k], x_send, x_recv.at[k], partner).start()

    def g5(k):
        drain(xoth.at[k], x_recv.at[k])
        rows = jnp.concatenate([ref[k, col].reshape(256, HALF) for ref in (xown, xoth) for col in range(2)], axis=1)
        gate = jnp.minimum(jnp.dot(rows, wg[...], preferred_element_type=F32), 7.0)
        lin = jnp.clip(jnp.dot(rows, wu[...], preferred_element_type=F32), -7.0, 7.0)
        sig = 0.5 * jnp.tanh(0.851 * gate) + 0.5
        hown[k] = (gate * sig * (lin + 1.0)).astype(BF)
        remote(hown.at[k], hoth.at[k], h_send, h_recv.at[k], partner).start()

    def d6(k):
        drain(hoth.at[k], h_recv.at[k])
        hidden = jnp.concatenate([hown[k], hoth[k]], axis=1)
        done = jnp.dot(hidden, wd[...], preferred_element_type=F32).astype(BF)
        for col in range(2):
            rows = done[:, col * HALF : (col + 1) * HALF].reshape(4, 4, CAP, HALF)
            for j in range(4):
                piece = rows[j] if col == 0 else rows[:, j]
                if j:
                    ysend[k, col, j - 1] = piece
                else:
                    r1buf[k, col, 0] = piece
            for j in (1, 3, 2):
                remote(
                    ysend.at[k, col, j - 1], r1buf.at[k, col, (-j) % 4], r1_send, r1_recv.at[k, col], far(col, j)
                ).start()

    def u7(k):
        for col in range(2):
            drain(ysend.at[k, col], r1_recv.at[k, col])
            rows = r1buf[k, col].reshape(256, HALF)
            sums = lax.dot_general(
                select(k, col, True), rows, (((0,), (0,)), ((), ())), preferred_element_type=F32
            )
            pacc[k, col] = sums[:BLK]
            for j in range(1, 4):
                r2send[k, col, j - 1] = sums[BLK * j : BLK * j + BLK].astype(BF)
            for j in (1, 3, 2):
                remote(
                    r2send.at[k, col, j - 1], r2buf.at[k, col, (-j) % 4 - 1], r2_send, r2_recv.at[k, col], peer(col, j)
                ).start()

    def r8(k):
        for col in range(2):
            drain(r2buf.at[k, col], r2_recv.at[k, col])
            total = pacc[k, col]
            for j in range(3):
                total = total + r2buf[k, col, j].astype(F32)
            if k:
                r3send[k, col] = total.astype(BF)
            else:
                pacc[0, col] = total
        if k:
            slot = (-k) % NZ
            remote(r3send.at[k], r3buf.at[slot], r3_send, r3_recv.at[slot], at(dz=k)).start()

    start_z()
    n = NZ
    order = ARRIVAL
    back = order[1:] + order[:1]
    s2(order[0])
    ready = False
    for i in range(n + 7):
        if i + 1 < n:
            s2(order[i + 1])
        if i < n:
            s3(order[i])
        if 0 <= i - 1 < n:
            x4(order[i - 1])
        if 0 <= i - 2 < n:
            if not ready:
                for copy in weights:
                    copy.wait()
                ready = True
            g5(order[i - 2])
        if 0 <= i - 3 < n:
            d6(order[i - 3])
        if 0 <= i - 5 < n:
            u7(order[i - 5])
        if 0 <= i - 6 < n:
            r8(order[i - 6])

    for col in range(2):
        total = pacc[0, col]
        for k in range(1, NZ):
            if col == 0:
                drain(r3buf.at[k], r3_recv.at[k])
            total = total + r3buf[k, col].astype(F32)
        out_ref[:, col * HALF : (col + 1) * HALF] = total.astype(BF)

    drain(own.at[pl.ds(1, 7)], z_send)
    drain(ybuf.at[:, :, pl.ds(1, 3)], s2_send)
    drain(sbuf, s3_send)
    drain(xown, x_send)
    drain(hown, h_send)
    drain(ysend, r1_send)
    drain(r2send, r2_send)
    drain(r3send.at[pl.ds(1, 7)], r3_send)


def shards(tokens, norm_gain, routing, route_logits, w_gate, w_up, w_down):
    vmem = pltpu.VMEM
    dma = pltpu.SemaphoreType.DMA
    return pl.pallas_call(
        kernel,
        name="routed_layer",
        out_shape=jax.ShapeDtypeStruct((BLK, 2 * HALF), BF),
        in_specs=[pl.BlockSpec(memory_space=pl.ANY)] * 7,
        out_specs=pl.BlockSpec(memory_space=vmem),
        scratch_shapes=[
            vmem((BLK, 1024), BF),
            vmem((1, 1024), F32),
            vmem((4, BLK), jnp.int32),
            vmem((4, BLK), F32),
            vmem((1024, 512), BF),
            vmem((1024, 512), BF),
            vmem((1024, 512), BF),
            vmem((NZ, 2, ROWS, HALF), BF),
            vmem((NZ, 2, 4, ROWS, HALF), BF),
            vmem((NZ, 2, 3, 4, CAP, HALF), BF),
            vmem((NZ, 2, 4, 4, CAP, HALF), BF),
            vmem((NZ, 2, 4, 4, CAP, HALF), BF),
            vmem((NZ, 256, 512), BF),
            vmem((NZ, 256, 512), BF),
            vmem((NZ, 2, 3, 4, CAP, HALF), BF),
            vmem((NZ, 2, 4, 4, CAP, HALF), BF),
            vmem((NZ, 2, BLK, HALF), F32),
            vmem((NZ, 2, 3, BLK, HALF), BF),
            vmem((NZ, 2, 3, BLK, HALF), BF),
            vmem((NZ, 2, BLK, HALF), BF),
            vmem((NZ, 2, BLK, HALF), BF),
            dma((4,)),
            dma((3, 2)),
            dma, dma((NZ,)),
            dma, dma((NZ, 2)),
            dma, dma((NZ, 2)),
            dma, dma((NZ,)),
            dma, dma((NZ,)),
            dma, dma((NZ, 2)),
            dma, dma((NZ, 2)),
            dma, dma((NZ,)),
        ],
        compiler_params=pltpu.CompilerParams(
            collective_id=0, has_side_effects=True, vmem_limit_bytes=60 * 1024 * 1024
        ),
    )(tokens, norm_gain.reshape(1, -1), routing.T, route_logits.T, w_gate[0], w_up[0], w_down[0])


def solution(mesh):
    return jax.shard_map(
        shards,
        mesh=mesh,
        in_specs=(
            P("ep", None),
            P(),
            P("ep", None),
            P("ep", None),
            P("ep", None, "tp"),
            P("ep", None, "tp"),
            P("ep", None, "tp"),
        ),
        out_specs=P("ep", "tp"),
        check_vma=False,
    )
```

time: 924 us -> 67.1 us (0.07)
  the two profiles are of different devices: /device:TPU:0 before, /device:TPU:2 now
where the time goes in v2:
time: 67.1 us; the launch traced here: 66.9 us
  Pallas kernels  65.6 us (98%)
  local copies, waits for them, and re-layouts  1.38 us (2%)
    pallas_call x1, Pallas kernels, shards(): pl.pallas_call(kernel, name='routed_layer', out_shape=jax.ShapeDtypeStruc...  65.6 us
    unnamed x1, local copies, waits for them, and re-layouts  1.38 us

profile of v2, /device:TPU:2, one launch (start us, length us, event | category | flops | bytes accessed | tf_op | source)
XLA Modules:
  0.0 66.9 jit_solution(12032101887103210208)
XLA Ops:
  0.0 65.6 %routed_layer.1 = bf16[32,512]{1,0:T(8,128)(2,1)} custom-call(bf16[32,1024]{1,0:T(8,128)(2,1)} %tok_hbm.1, f32[1,1024]{1,0:T(1,128)} %bitcast.9, s32[4,32]{1,0:T(4,128)} %bitcast.10, f32[4,32]{1,0:T(4,128)} %bitcast.11, bf16[1024,512]{1,0:T(8,128)(2,1)} %bitcast.6, bf16[1024,512]{1,0:T(8,128)(2,1)} %bitcast.7, bf16[1024,512]{1,0:T(8,128)(2,1)} %bitcast.8), custom_call_target="tpu_custom_call" | custom-call | tf_op jit(solution)/shard_map/routed_layer/pallas_call | solution.py:285
  65.6 1.4 %copy.9 = bf16[32,512]{1,0:T(8,128)(2,1)} copy(bf16[32,512]{1,0:T(8,128)(2,1)} %routed_layer.1) | data formatting | bytes 65536

commit v3 on v2

--- a/solution.py
+++ b/solution.py
@@ -14,7 +14,19 @@
 EPS = 1e-05
 BF = jnp.bfloat16
 F32 = jnp.float32
-ARRIVAL = (0, 1, 7, 2, 6, 3, 5, 4)
+SEQ = (
+    (0, 0, 1), (0, 0, 0), (0, 7, 1), (0, 7, 0), (1, 0, 1), (1, 0, 0), (0, 6, 1), (0, 2, 0),
+    (0, 1, 1), (0, 1, 0), (1, 7, 1), (1, 7, 0), (0, 6, 0), (0, 3, 0), (0, 3, 1), (0, 5, 0),
+    (0, 2, 1), (2, 0, 0), (1, 1, 0), (0, 4, 1), (0, 4, 0), (3, 0, 0), (1, 1, 1), (2, 7, 0),
+    (0, 5, 1), (1, 3, 1), (1, 3, 0), (1, 6, 1), (1, 6, 0), (3, 7, 0), (1, 4, 0), (1, 4, 1),
+    (2, 1, 0), (1, 5, 1), (1, 2, 1), (1, 5, 0), (1, 2, 0), (2, 3, 0), (4, 0, 0), (3, 1, 0),
+    (4, 7, 0), (2, 6, 0), (2, 4, 0), (3, 3, 0), (4, 1, 0), (2, 5, 0), (3, 6, 0), (3, 4, 0),
+    (4, 3, 0), (2, 2, 0), (3, 5, 0), (4, 6, 0), (4, 4, 0), (3, 2, 0), (4, 5, 0), (5, 3, 0),
+    (4, 2, 0), (5, 3, 1), (5, 4, 1), (5, 4, 0), (5, 1, 0), (5, 7, 1), (5, 5, 1), (5, 5, 0),
+    (5, 1, 1), (5, 7, 0), (5, 6, 1), (5, 2, 0), (5, 6, 0), (5, 2, 1), (5, 0, 1), (6, 4, 1),
+    (6, 4, 0), (6, 3, 1), (5, 0, 0), (6, 3, 0), (6, 5, 1), (6, 5, 0), (6, 7, 0), (6, 6, 1),
+    (6, 2, 0), (6, 2, 1), (6, 6, 0), (6, 0, 1), (6, 1, 1), (6, 1, 0), (6, 0, 0), (6, 7, 1),
+)
 
 
 def iota(shape, dim):
@@ -71,8 +83,6 @@
             weights.append(
                 pltpu.make_async_copy(src.at[pl.ds(start, 512)], dst.at[pl.ds(part * 512, 512)], w_sem.at[i, part])
             )
-    for copy in weights:
-        copy.start()
 
     barrier = pltpu.get_barrier_semaphore()
     friends = [at(dz=k) for k in range(1, NZ)] + [at(dy=j) for j in range(1, NY)] + [at(dx=j) for j in range(1, NX)]
@@ -82,6 +92,8 @@
 
     for copy in small:
         copy.wait()
+    for copy in weights:
+        copy.start()
 
     full = tok[...].astype(F32)
     scale = lax.rsqrt(jnp.mean(full * full, axis=-1, keepdims=True) + EPS)
@@ -129,14 +141,16 @@
             slot = (-k) % NZ
             remote(own.at[k], ybuf.at[slot, :, 0], z_send, z_recv.at[slot], at(dz=k)).start()
 
-    def s2(k):
-        if k:
+    seen = set()
+
+    def s2(k, col):
+        if k and k not in seen:
             drain(own.at[k], z_recv.at[k])
+            seen.add(k)
         for j in (1, 3, 2):
-            for col in range(2):
-                remote(
-                    ybuf.at[k, col, 0], ybuf.at[k, col, (-j) % 4], s2_send, s2_recv.at[k, col], peer(col, j)
-                ).start()
+            remote(
+                ybuf.at[k, col, 0], ybuf.at[k, col, (-j) % 4], s2_send, s2_recv.at[k, col], peer(col, j)
+            ).start()
 
     lanes = iota((8, 128), 1) // BLK
     sixty = iota((64, 128), 0)
@@ -157,30 +171,33 @@
             parts.append(jnp.where(sixty == wanted, value, 0.0).astype(BF))
         return jnp.concatenate(parts, axis=0)
 
-    def s3(k):
-        for col in range(2):
-            drain(ybuf.at[k, col, pl.ds(1, 3)], s2_recv.at[k, col])
-            rows = ybuf[k, col, :, :BLK, :].reshape(128, HALF)
-            packed = jnp.dot(select(k, col, False), rows, preferred_element_type=F32).astype(BF)
-            for j in range(4):
-                piece = packed[64 * j : 64 * j + 64].reshape(4, CAP, HALF)
-                if j:
-                    sbuf[k, col, j - 1] = piece
-                elif col == 0:
-                    xown[k, 0, 0] = piece
-                else:
-                    xown[k, 1, :, 0] = piece
-            for j in (1, 3, 2):
-                slot = (-j) % 4
-                dst = xown.at[k, 0, slot] if col == 0 else xown.at[k, 1, :, slot]
-                remote(sbuf.at[k, col, j - 1], dst, s3_send, s3_recv.at[k, col], far(col, j)).start()
-
-    def x4(k):
+    def s3(k, col):
+        drain(ybuf.at[k, col, pl.ds(1, 3)], s2_recv.at[k, col])
+        rows = ybuf[k, col, :, :BLK, :].reshape(128, HALF)
+        packed = jnp.dot(select(k, col, False), rows, preferred_element_type=F32).astype(BF)
+        for j in range(4):
+            piece = packed[64 * j : 64 * j + 64].reshape(4, CAP, HALF)
+            if j:
+                sbuf[k, col, j - 1] = piece
+            elif col == 0:
+                xown[k, 0, 0] = piece
+            else:
+                xown[k, 1, :, 0] = piece
+        for j in (1, 3, 2):
+            slot = (-j) % 4
+            dst = xown.at[k, 0, slot] if col == 0 else xown.at[k, 1, :, slot]
+            remote(sbuf.at[k, col, j - 1], dst, s3_send, s3_recv.at[k, col], far(col, j)).start()
+
+    def x4(k, _):
         for col in range(2):
             drain(sbuf.at[k, col], s3_recv.at[k, col])
         remote(xown.at[k], xoth.at[k], x_send, x_recv.at[k], partner).start()
 
-    def g5(k):
+    def g5(k, _):
+        if "w" not in seen:
+            seen.add("w")
+            for copy in weights:
+                copy.wait()
         drain(xoth.at[k], x_recv.at[k])
         rows = jnp.concatenate([ref[k, col].reshape(256, HALF) for ref in (xown, xoth) for col in range(2)], axis=1)
         gate = jnp.minimum(jnp.dot(rows, wg[...], preferred_element_type=F32), 7.0)
@@ -189,7 +206,7 @@
         hown[k] = (gate * sig * (lin + 1.0)).astype(BF)
         remote(hown.at[k], hoth.at[k], h_send, h_recv.at[k], partner).start()
 
-    def d6(k):
+    def d6(k, _):
         drain(hoth.at[k], h_recv.at[k])
         hidden = jnp.concatenate([hown[k], hoth[k]], axis=1)
         done = jnp.dot(hidden, wd[...], preferred_element_type=F32).astype(BF)
@@ -206,60 +223,36 @@
                     ysend.at[k, col, j - 1], r1buf.at[k, col, (-j) % 4], r1_send, r1_recv.at[k, col], far(col, j)
                 ).start()
 
-    def u7(k):
-        for col in range(2):
-            drain(ysend.at[k, col], r1_recv.at[k, col])
-            rows = r1buf[k, col].reshape(256, HALF)
-            sums = lax.dot_general(
-                select(k, col, True), rows, (((0,), (0,)), ((), ())), preferred_element_type=F32
-            )
-            pacc[k, col] = sums[:BLK]
-            for j in range(1, 4):
-                r2send[k, col, j - 1] = sums[BLK * j : BLK * j + BLK].astype(BF)
-            for j in (1, 3, 2):
-                remote(
-                    r2send.at[k, col, j - 1], r2buf.at[k, col, (-j) % 4 - 1], r2_send, r2_recv.at[k, col], peer(col, j)
-                ).start()
-
-    def r8(k):
-        for col in range(2):
-            drain(r2buf.at[k, col], r2_recv.at[k, col])
-            total = pacc[k, col]
-            for j in range(3):
-                total = total + r2buf[k, col, j].astype(F32)
-            if k:
-                r3send[k, col] = total.astype(BF)
-            else:
-                pacc[0, col] = total
+    def u7(k, col):
+        drain(ysend.at[k, col], r1_recv.at[k, col])
+        rows = r1buf[k, col].reshape(256, HALF)
+        sums = lax.dot_general(select(k, col, True), rows, (((0,), (0,)), ((), ())), preferred_element_type=F32)
+        pacc[k, col] = sums[:BLK]
+        for j in range(1, 4):
+            r2send[k, col, j - 1] = sums[BLK * j : BLK * j + BLK].astype(BF)
+        for j in (1, 3, 2):
+            remote(
+                r2send.at[k, col, j - 1], r2buf.at[k, col, (-j) % 4 - 1], r2_send, r2_recv.at[k, col], peer(col, j)
+            ).start()
+
+    def r8(k, col):
+        drain(r2buf.at[k, col], r2_recv.at[k, col])
+        total = pacc[k, col]
+        for j in range(3):
+            total = total + r2buf[k, col, j].astype(F32)
         if k:
+            r3send[k, col] = total.astype(BF)
+        else:
+            pacc[0, col] = total
+        if k and ("r", k) in seen:
             slot = (-k) % NZ
             remote(r3send.at[k], r3buf.at[slot], r3_send, r3_recv.at[slot], at(dz=k)).start()
+        seen.add(("r", k))
 
     start_z()
-    n = NZ
-    order = ARRIVAL
-    back = order[1:] + order[:1]
-    s2(order[0])
-    ready = False
-    for i in range(n + 7):
-        if i + 1 < n:
-            s2(order[i + 1])
-        if i < n:
-            s3(order[i])
-        if 0 <= i - 1 < n:
-            x4(order[i - 1])
-        if 0 <= i - 2 < n:
-            if not ready:
-                for copy in weights:
-                    copy.wait()
-                ready = True
-            g5(order[i - 2])
-        if 0 <= i - 3 < n:
-            d6(order[i - 3])
-        if 0 <= i - 5 < n:
-            u7(order[i - 5])
-        if 0 <= i - 6 < n:
-            r8(order[i - 6])
+    steps = (s2, s3, x4, g5, d6, u7, r8)
+    for step, k, col in SEQ:
+        steps[step](k, col)
 
     for col in range(2):
         total = pacc[0, col]
@@ -285,7 +278,7 @@
     return pl.pallas_call(
         kernel,
         name="routed_layer",
-        out_shape=jax.ShapeDtypeStruct((BLK, 2 * HALF), BF),
+        out_shape=vmem((BLK, 2 * HALF), BF),
         in_specs=[pl.BlockSpec(memory_space=pl.ANY)] * 7,
         out_specs=pl.BlockSpec(memory_space=vmem),
         scratch_shapes=[

time: 67.1 us -> 57.1 us (0.85)
  the two profiles are of different devices: /device:TPU:2 before, /device:TPU:1 now
where the time goes in v3:
time: 57.1 us; the launch traced here: 57 us
  Pallas kernels  56.3 us (99%)
  local copies, waits for them, and re-layouts  0.62 us (1%)
    pallas_call x1, Pallas kernels, shards(): pl.pallas_call(kernel, name='routed_layer', out_shape=vmem((BLK, 2 * HALF...  56.3 us

profile of v3, /device:TPU:1, one launch (start us, length us, event | category | flops | bytes accessed | tf_op | source)
XLA Modules:
  0.0 57.0 jit_solution(5256953611430135534)
XLA Ops:
  0.0 56.3 %routed_layer.1 = bf16[32,512]{1,0:T(8,128)(2,1)S(1)} custom-call(bf16[32,1024]{1,0:T(8,128)(2,1)} %tok_hbm.1, f32[1,1024]{1,0:T(1,128)} %bitcast.9, s32[4,32]{1,0:T(4,128)} %bitcast.10, f32[4,32]{1,0:T(4,128)} %bitcast.11, bf16[1024,512]{1,0:T(8,128)(2,1)} %bitcast.6, bf16[1024,512]{1,0:T(8,128)(2,1)} %bitcast.7, bf16[1024,512]{1,0:T(8,128)(2,1)} %bitcast.8), custom_call_target="tpu_custom_call" | custom-call | tf_op jit(solution)/shard_map/routed_layer/pallas_call | solution.py:278
  56.3 0.6 %copy.9 = bf16[32,512]{1,0:T(8,128)(2,1)} copy(bf16[32,512]{1,0:T(8,128)(2,1)S(1)} %routed_layer.1) | data formatting | bytes 65536

commit v4 on v3

v4 whole, which is shorter than its diff:
```python
import jax
import jax.numpy as jnp
from jax import lax
from jax.experimental import pallas as pl
from jax.experimental.pallas import tpu as pltpu
from jax.sharding import PartitionSpec as P

MESH = pl.DeviceIdType.MESH
NX, NY, NZ = 4, 4, 8
CAP = 16
BLK = 32
HALF = 256
EPS = 1e-05
BF = jnp.bfloat16
F32 = jnp.float32
PAIRS = ((1, 7), (0, 2), (6, 3), (5, 4))
NEAR = (1, 7)
DISTANT = (2, 6, 3, 5, 4)
OWNER = {k: c for pair in PAIRS for c, k in enumerate(pair)}
PLACE = {k: i for i, pair in enumerate(PAIRS) for k in pair}
SEQ = (
    (0, 0, 0), (2, 7, 1), (2, 1, 0), (2, 1, 1), (2, 0, 1), (2, 0, 0), (1, 6, 1), (1, 5, 0),
    (1, 5, 1), (1, 4, 1), (1, 4, 0), (1, 3, 0), (2, 7, 0), (1, 6, 0), (1, 2, 1), (2, 6, 1),
    (1, 2, 0), (1, 3, 1), (2, 5, 0), (2, 5, 1), (2, 4, 0), (2, 6, 0), (2, 4, 1), (2, 3, 0),
    (2, 2, 1), (3, 0, 0), (2, 3, 1), (3, 0, 1), (2, 2, 0), (4, 0, 0), (4, 0, 1), (3, 3, 0),
    (3, 3, 1), (4, 3, 1), (4, 3, 0), (3, 2, 0), (3, 2, 1), (4, 2, 1), (4, 2, 0), (3, 1, 0),
    (3, 1, 1), (5, 4, 1), (5, 4, 0), (4, 1, 0), (5, 5, 1), (4, 1, 1), (5, 3, 0), (5, 3, 1),
    (5, 5, 0), (6, 4, 1), (5, 6, 1), (5, 6, 0), (6, 4, 0), (5, 1, 0), (5, 2, 1), (5, 2, 0),
    (6, 5, 1), (6, 3, 0), (5, 1, 1), (6, 5, 0), (6, 3, 1), (5, 7, 0), (5, 0, 0), (5, 0, 1),
    (6, 6, 1), (6, 6, 0), (7, 0, 0), (5, 7, 1), (7, 0, 1), (6, 2, 0), (6, 2, 1),
)


def iota(shape, dim):
    return lax.broadcasted_iota(jnp.int32, shape, dim)


def kernel(
    tok_hbm, gain_hbm, ids_hbm, log_hbm, wg_hbm, wu_hbm, wd_hbm, out_ref,
    tok, gain, ids, logits, wg, wu, wd,
    lsend, lmeta, msrc, mtab, pbuf, sbuf, xbuf, hid, ysend, r1buf, eacc, pacc, r2send, r2buf, r3send, r3buf,
    in_sem, w_sem, w_send, w_recv, l_send, l_recv, m_send, m_recv, z_send, z_recv, s2_send, s2_recv,
    s3_send, x_recv, r1_send, r1_recv, r1_own, r2_send, r2_recv, r3_send, r3_recv,
):
    ep = lax.axis_index("ep")
    c = lax.axis_index("tp")
    x = lax.rem(ep, NX)
    y = lax.rem(ep // NX, NY)
    z = ep // (NX * NY)

    def at(dx=0, dy=0, dz=0, core=None):
        px = lax.rem(x + dx, NX)
        py = lax.rem(y + dy, NY)
        pz = lax.rem(z + dz, NZ)
        return ((pz * NY + py) * NX + px, c if core is None else core)

    partner = (ep, 1 - c)

    def peer(col, j):
        return at(dy=j) if col == 0 else at(dx=j)

    def far(col, j, dz, core):
        return at(dx=j, dz=dz, core=core) if col == 0 else at(dy=j, dz=dz, core=core)

    def remote(src, dst, send, recv, device):
        pltpu.make_async_remote_copy(
            src_ref=src, dst_ref=dst, send_sem=send, recv_sem=recv, device_id=device, device_id_type=MESH
        ).start()

    def drain(ref, sem):
        pltpu.make_async_copy(ref, ref, sem).wait()

    small = [
        pltpu.make_async_copy(tok_hbm, tok, in_sem.at[0]),
        pltpu.make_async_copy(gain_hbm, gain, in_sem.at[1]),
        pltpu.make_async_copy(ids_hbm, ids, in_sem.at[2]),
        pltpu.make_async_copy(log_hbm, logits, in_sem.at[3]),
    ]
    for copy in small:
        copy.start()

    barrier = pltpu.get_barrier_semaphore()
    both = (0, 1)
    friends = [partner]
    friends += [at(dy=j, core=o) for j in range(1, NY) for o in both]
    friends += [at(dx=j, core=o) for j in range(1, NX) for o in both]
    for k in NEAR:
        friends += [at(dz=k, core=o) for o in both]
        friends += [at(dy=j, dz=k, core=o) for j in range(1, NY) for o in both]
        friends += [at(dx=j, dz=k, core=o) for j in range(1, NX) for o in both]
    friends += [at(dz=k) for k in DISTANT]
    for friend in friends:
        pl.semaphore_signal(barrier, inc=1, device_id=friend, device_id_type=MESH)

    for copy in small:
        copy.wait()
    weights = [pltpu.make_async_copy(src, dst.at[c], w_sem.at[i]) for i, (src, dst) in enumerate(((wg_hbm, wg), (wu_hbm, wu), (wd_hbm, wd)))]
    for copy in weights:
        copy.start()

    full = tok[...].astype(F32)
    scale = lax.rsqrt(jnp.mean(full * full, axis=-1, keepdims=True) + EPS)
    mine = pl.ds(pl.multiple_of(c * 512, 512), 512)
    normed = (tok[:, mine].astype(F32) * scale * gain[:, mine]).astype(BF)
    for col in range(2):
        pbuf[0, col, 0] = normed[:, col * HALF : (col + 1) * HALF]

    spread = (lax.rem(iota((BLK, 128), 1), BLK) == iota((BLK, 128), 0)).astype(BF)
    raw = logits[...]
    shifted = jnp.exp(raw - jnp.max(raw, axis=0, keepdims=True))
    probs = shifted / jnp.sum(shifted, axis=0, keepdims=True)
    ids_l = jnp.dot(ids[...].astype(F32).astype(BF), spread, preferred_element_type=F32)
    probs_l = jnp.dot(probs.astype(BF), spread, preferred_element_type=F32)
    row = iota((128, 128), 0)
    lane = iota((128, 128), 1)
    plane = lax.rem(z + lax.rem(row // 8, 2) * 4 + lane // BLK, NZ)
    group = lax.rem(row // 16, 4)
    near = lax.rem(row, 4)
    route_b = row < 64
    ex = lax.rem(x + jnp.where(route_b, near, group), NX)
    ey = lax.rem(y + jnp.where(route_b, group, near), NY)
    expert = (plane * 16 + ey * NX + ex).astype(F32)
    named = jnp.zeros((128, 128), F32)
    weight = jnp.zeros((128, 128), F32)
    for q in range(4):
        hit = expert == ids_l[q : q + 1, :]
        named = jnp.where(hit, 1.0, named)
        weight = jnp.where(hit, probs_l[q : q + 1, :], weight)
    before = ((row // BLK == lane // BLK) & (row < lane)).astype(BF)
    place = jnp.dot(named.astype(BF), before, preferred_element_type=F32)
    place = jnp.where(named > 0, place, -128.0)
    meta = jnp.where(lax.rem(row, 8) < 4, place, weight).astype(BF)
    for col in range(2):
        for g in range(4):
            for hi in range(2):
                start = col * 64 + g * 16 + hi * 8
                tile = meta[start : start + 8, :]
                if g:
                    lsend[col, g, hi] = tile
                else:
                    lmeta[col, 0, hi] = tile

    pl.semaphore_wait(barrier, len(friends))

    for col in range(2):
        for j in (1, 3, 2):
            remote(lsend.at[col, j], lmeta.at[col, (-j) % 4], l_send, l_recv.at[col], peer(col, j))
            remote(pbuf.at[0, col, 0], pbuf.at[0, col, (-j) % 4], s2_send, s2_recv.at[0, col], peer(col, j))
    for k in DISTANT:
        slot = (-k) % NZ
        remote(pbuf.at[0, :, 0], pbuf.at[slot, :, 0], z_send, z_recv.at[slot], at(dz=k))
    for i, (src, dst) in enumerate(((wg_hbm, wg), (wu_hbm, wu), (wd_hbm, wd))):
        remote(src, dst.at[c], w_send, w_recv.at[i], partner)

    seen = set()

    def once(key):
        if key in seen:
            return False
        seen.add(key)
        return True

    def mb(k, col):
        lanes = iota((8, 128), 1) // BLK
        base = jnp.where(iota((8, 128), 0) < 4, lanes * CAP, 0).astype(F32)
        for col in range(2):
            drain(lsend.at[col, pl.ds(1, 3)], l_recv.at[col])
            for hi in range(2):
                t = [lmeta[col, s, hi].astype(F32) for s in range(4)]
                for lo in range(4):
                    turned = [t[s] if s == lo else pltpu.roll(t[s], BLK * ((s - lo) % 4), 1) for s in range(4)]
                    m = jnp.where(
                        lanes < 2, jnp.where(lanes == 0, turned[0], turned[1]), jnp.where(lanes == 2, turned[2], turned[3])
                    )
                    msrc[hi * 4 + lo, col] = (m + base).astype(BF)
        for k in DISTANT:
            slot = (-k) % NZ
            remote(msrc.at[k], mtab.at[slot], m_send, m_recv.at[slot], at(dz=k))

    def s2(k, col):
        if once(("z", k)):
            drain(pbuf.at[k, :, 0], z_recv.at[k])
        for j in (1, 3, 2):
            remote(pbuf.at[k, col, 0], pbuf.at[k, col, (-j) % 4], s2_send, s2_recv.at[k, col], peer(col, j))

    def table(k, col):
        if k == 0 or k in NEAR:
            return msrc[k, col].astype(F32)
        return mtab[k, col].astype(F32)

    def select(k, col, weighted):
        m = table(k, col)
        sixty = iota((64, 128), 0).astype(F32)
        parts = []
        for j in range(4):
            value = m[4 + j : 5 + j, :] if weighted else 1.0
            parts.append(jnp.where(sixty == m[j : j + 1, :], value, 0.0).astype(BF))
        return jnp.concatenate(parts, axis=0)

    def s3(k, col):
        source = 0 if k in NEAR else k
        if once(("s2", source, col)):
            drain(pbuf.at[source, col, pl.ds(1, 3)], s2_recv.at[source, col])
        if k in DISTANT and once(("m", k)):
            drain(mtab.at[k], m_recv.at[k])
        rows = pbuf[source, col].reshape(128, HALF)
        packed = jnp.dot(select(k, col, False), rows, preferred_element_type=F32).astype(BF)
        there = (-k) % NZ if k in NEAR else k
        i, core = PLACE[there], OWNER[there]

        def target(slot):
            return xbuf.at[i, c, 0, slot] if col == 0 else xbuf.at[i, c, 1, :, slot]

        pieces = [packed[64 * j : 64 * j + 64].reshape(4, CAP, HALF) for j in range(4)]
        for j in range(4):
            if j or k in NEAR:
                sbuf[k, col, j] = pieces[j]
        for j in (1, 3, 2, 0) if k in NEAR else (1, 3, 2):
            device = far(col, j, k if k in NEAR else 0, core)
            remote(sbuf.at[k, col, j], target((-j) % 4), s3_send.at[1 if k in NEAR else 0], x_recv.at[i, c, col], device)
        if k not in NEAR:

            @pl.when(c == core)
            def _():
                if col == 0:
                    xbuf[i, c, 0, 0] = pieces[0]
                else:
                    xbuf[i, c, 1, :, 0] = pieces[0]

            @pl.when(c != core)
            def _():
                sbuf[k, col, 0] = pieces[0]
                remote(sbuf.at[k, col, 0], target(0), s3_send.at[2], x_recv.at[i, c, col], partner)

    def ga(i, h):
        if once(("x", i)):
            for col in range(2):
                if PAIRS[i][0] in NEAR:
                    drain(sbuf.at[0, 0], x_recv.at[i, c, col])
                else:
                    drain(sbuf.at[0, 0, pl.ds(1, 3)], x_recv.at[i, c, col])
                drain(sbuf.at[0, 0], x_recv.at[i, 1 - c, col])
        if once("w"):
            for n in range(2):
                weights[n].wait()
                drain(wg.at[0], w_recv.at[n])
        rows = jnp.concatenate([xbuf[i, s, col].reshape(256, HALF) for s in range(2) for col in range(2)], axis=1)
        gate = jnp.minimum(jnp.dot(rows, wg[h], preferred_element_type=F32), 7.0)
        lin = jnp.clip(jnp.dot(rows, wu[h], preferred_element_type=F32), -7.0, 7.0)
        sig = 0.5 * jnp.tanh(0.851 * gate) + 0.5
        hid[i, h] = (gate * sig * (lin + 1.0)).astype(BF)

    def db(i, h):
        if once("d"):
            weights[2].wait()
            drain(wd.at[0], w_recv.at[2])
        hidden = jnp.concatenate([hid[i, 0], hid[i, 1]], axis=1)
        done = jnp.dot(hidden, wd[h], preferred_element_type=F32).astype(BF)
        k0, k1 = PAIRS[i]
        close = k0 in NEAR
        k = k0 + c * (k1 - k0)
        there = lax.rem(NZ - k, NZ) if close else k
        for col in range(2):
            rows = done[:, col * HALF : (col + 1) * HALF].reshape(4, 4, CAP, HALF)
            pieces = [rows[j] if col == 0 else rows[:, j] for j in range(4)]
            for j in range(4):
                if j or close:
                    ysend[i, h, col, j] = pieces[j]
            for j in (1, 3, 2, 0) if close else (1, 3, 2):
                device = far(col, j, k if close else 0, h)
                remote(
                    ysend.at[i, h, col, j], r1buf.at[there, col, (-j) % 4], r1_send.at[1 if close else 0],
                    r1_recv.at[there, col], device,
                )
            if not close:

                @pl.when(c == h)
                def _():
                    r1buf[there, col, 0] = pieces[0]

                @pl.when(c != h)
                def _():
                    ysend[i, h, col, 0] = pieces[0]
                    remote(
                        ysend.at[i, h, col, 0], r1buf.at[there, col, 0], r1_send.at[2], r1_own.at[there, col], partner
                    )

    def to_line(k, col, sums):
        pacc[k, col] = sums[:BLK]
        for j in range(1, 4):
            r2send[k, col, j - 1] = sums[BLK * j : BLK * j + BLK].astype(BF)
        for j in (1, 3, 2):
            remote(
                r2send.at[k, col, j - 1], r2buf.at[k, col, (-j) % 4 - 1], r2_send.at[1 if k else 0],
                r2_recv.at[k, col], peer(col, j),
            )

    def u7(k, col):
        if k in NEAR:
            drain(ysend.at[0, 0, 0], r1_recv.at[k, col])
        else:
            drain(ysend.at[0, 0, 0, pl.ds(1, 3)], r1_recv.at[k, col])

            @pl.when(c != OWNER[k])
            def _():
                drain(ysend.at[0, 0, 0, 0], r1_own.at[k, col])

        rows = r1buf[k, col].reshape(256, HALF)
        sums = lax.dot_general(select(k, col, True), rows, (((0,), (0,)), ((), ())), preferred_element_type=F32)
        if k == 0 or k in NEAR:
            if once(("e", col)):
                eacc[col] = sums
            else:
                eacc[col] += sums
        else:
            to_line(k, col, sums)

    def e2(k, col):
        to_line(0, col, eacc[col])

    def r8(k, col):
        drain(r2buf.at[k, col], r2_recv.at[k, col])
        total = pacc[k, col]
        for j in range(3):
            total = total + r2buf[k, col, j].astype(F32)
        slot = (-k) % NZ
        r3send[k, col] = total.astype(BF)
        remote(r3send.at[k, col], r3buf.at[slot, col], r3_send, r3_recv.at[slot, col], at(dz=k))

    steps = (mb, s2, s3, ga, db, u7, r8, e2)
    for step, k, col in SEQ:
        pl.when(c < 2)(lambda step=step, k=k, col=col: steps[step](k, col))

    for col in range(2):
        total = pacc[0, col]
        for k in DISTANT:
            drain(r3buf.at[k, col], r3_recv.at[k, col])
            total = total + r3buf[k, col].astype(F32)
        drain(r2buf.at[0, col], r2_recv.at[0, col])
        for j in range(3):
            total = total + r2buf[0, col, j].astype(F32)
        out_ref[:, col * HALF : (col + 1) * HALF] = total.astype(BF)

    six = pl.ds(0, 6)
    five = pl.ds(0, 5)
    three = pl.ds(0, 3)
    rest = pl.ds(1, 3)
    drain(lsend.at[:, rest], l_send)
    drain(pbuf.at[five, :, 0], z_send)
    drain(wg.at[0], w_send)
    drain(wu.at[0], w_send)
    drain(wd.at[0], w_send)
    drain(msrc.at[five], m_send)
    drain(pbuf.at[six, :, rest], s2_send)
    drain(sbuf.at[six, :, rest], s3_send.at[0])
    drain(sbuf.at[pl.ds(0, 2)], s3_send.at[1])
    drain(sbuf.at[three, :, 0], s3_send.at[2])
    drain(ysend.at[three, :, :, rest], r1_send.at[0])
    drain(ysend.at[0], r1_send.at[1])
    drain(ysend.at[three, 0, :, 0], r1_send.at[2])
    drain(r2send.at[0], r2_send.at[0])
    drain(r2send.at[five], r2_send.at[1])
    drain(r3send.at[five], r3_send)


def shards(tokens, norm_gain, routing, route_logits, w_gate, w_up, w_down):
    vmem = pltpu.VMEM
    dma = pltpu.SemaphoreType.DMA
    return pl.pallas_call(
        kernel,
        name="routed_layer",
        out_shape=vmem((BLK, 2 * HALF), BF),
        in_specs=[pl.BlockSpec(memory_space=pl.ANY)] * 7,
        out_specs=pl.BlockSpec(memory_space=vmem),
        scratch_shapes=[
            vmem((BLK, 1024), BF),
            vmem((1, 1024), F32),
            vmem((4, BLK), jnp.int32),
            vmem((4, BLK), F32),
            vmem((2, 1024, 512), BF),
            vmem((2, 1024, 512), BF),
            vmem((2, 1024, 512), BF),
            vmem((2, 4, 2, 8, 128), BF),
            vmem((2, 4, 2, 8, 128), BF),
            vmem((NZ, 2, 8, 128), BF),
            vmem((NZ, 2, 8, 128), BF),
            vmem((NZ, 2, 4, BLK, HALF), BF),
            vmem((NZ, 2, 4, 4, CAP, HALF), BF),
            vmem((4, 2, 2, 4, 4, CAP, HALF), BF),
            vmem((4, 2, 256, 512), BF),
            vmem((4, 2, 2, 4, 4, CAP, HALF), BF),
            vmem((NZ, 2, 4, 4, CAP, HALF), BF),
            vmem((2, 128, HALF), F32),
            vmem((NZ, 2, BLK, HALF), F32),
            vmem((NZ, 2, 3, BLK, HALF), BF),
            vmem((NZ, 2, 3, BLK, HALF), BF),
            vmem((NZ, 2, BLK, HALF), BF),
            vmem((NZ, 2, BLK, HALF), BF),
            dma((4,)),
            dma((3,)),
            dma, dma((3,)),
            dma, dma((2,)),
            dma, dma((NZ,)),
            dma, dma((NZ,)),
            dma, dma((NZ, 2)),
            dma((3,)), dma((4, 2, 2)),
            dma((3,)), dma((NZ, 2)), dma((NZ, 2)),
            dma((2,)), dma((NZ, 2)),
            dma, dma((NZ, 2)),
        ],
        compiler_params=pltpu.CompilerParams(
            collective_id=0, has_side_effects=True, vmem_limit_bytes=60 * 1024 * 1024
        ),
    )(tokens, norm_gain.reshape(1, -1), routing.T, route_logits.T, w_gate[0], w_up[0], w_down[0])


def solution(mesh):
    return jax.shard_map(
        shards,
        mesh=mesh,
        in_specs=(
            P("ep", None),
            P(),
            P("ep", None),
            P("ep", None),
            P("ep", None, "tp"),
            P("ep", None, "tp"),
            P("ep", None, "tp"),
        ),
        out_specs=P("ep", "tp"),
        check_vma=False,
    )
```

time: 57.1 us -> 55.3 us (0.968)
  Pallas kernels: 56.3 us -> 54.3 us
    pallas_call x1, Pallas kernels: 56.3 us -> 54.3 us  [shards(): pl.pallas_call(kernel, name='routed_layer', out_shape=vmem((BLK, 2 * HALF...]
where the time goes in v4:
time: 55.3 us; the launch traced here: 55 us
  Pallas kernels  54.3 us (98%)
  local copies, waits for them, and re-layouts  0.62 us (1%)
    pallas_call x1, Pallas kernels, shards(): pl.pallas_call(kernel, name='routed_layer', out_shape=vmem((BLK, 2 * HALF...  54.3 us

profile of v4, /device:TPU:1, one launch (start us, length us, event | category | flops | bytes accessed | tf_op | source)
XLA Modules:
  0.0 55.0 jit_solution(7539417336758139421)
XLA Ops:
  0.0 54.3 %routed_layer.1 = bf16[32,512]{1,0:T(8,128)(2,1)S(1)} custom-call(bf16[32,1024]{1,0:T(8,128)(2,1)} %tok_hbm.1, f32[1,1024]{1,0:T(1,128)} %bitcast.9, s32[4,32]{1,0:T(4,128)} %bitcast.10, f32[4,32]{1,0:T(4,128)} %bitcast.11, bf16[1024,512]{1,0:T(8,128)(2,1)} %bitcast.6, bf16[1024,512]{1,0:T(8,128)(2,1)} %bitcast.7, bf16[1024,512]{1,0:T(8,128)(2,1)} %bitcast.8), custom_call_target="tpu_custom_call" | custom-call | tf_op jit(solution)/shard_map/routed_layer/pallas_call | solution.py:369
  54.3 0.6 %copy.9 = bf16[32,512]{1,0:T(8,128)(2,1)} copy(bf16[32,512]{1,0:T(8,128)(2,1)S(1)} %routed_layer.1) | data formatting | bytes 65536

commit v5 on v4

--- a/solution.py
+++ b/solution.py
@@ -13,21 +13,28 @@
 EPS = 1e-05
 BF = jnp.bfloat16
 F32 = jnp.float32
-PAIRS = ((1, 7), (0, 2), (6, 3), (5, 4))
-NEAR = (1, 7)
-DISTANT = (2, 6, 3, 5, 4)
+PAIRS = ((1, 0), (7, 2), (6, 3), (5, 4))
+NEAR = ()
+DISTANT = tuple(k for k in (1, 7, 2, 6, 3, 5, 4) if k not in NEAR)
+NFAR = len(DISTANT)
+BUNDLE = (3, 5)
+SINGLE = tuple(k for k in DISTANT if k not in BUNDLE)
+FAR = {k: n for n, k in enumerate(DISTANT)}
+LINED = {k: n for n, k in enumerate((0,) + DISTANT)}
+ALONE = {k: n for n, k in enumerate((0,) + SINGLE)}
 OWNER = {k: c for pair in PAIRS for c, k in enumerate(pair)}
 PLACE = {k: i for i, pair in enumerate(PAIRS) for k in pair}
 SEQ = (
-    (0, 0, 0), (2, 7, 1), (2, 1, 0), (2, 1, 1), (2, 0, 1), (2, 0, 0), (1, 6, 1), (1, 5, 0),
-    (1, 5, 1), (1, 4, 1), (1, 4, 0), (1, 3, 0), (2, 7, 0), (1, 6, 0), (1, 2, 1), (2, 6, 1),
-    (1, 2, 0), (1, 3, 1), (2, 5, 0), (2, 5, 1), (2, 4, 0), (2, 6, 0), (2, 4, 1), (2, 3, 0),
-    (2, 2, 1), (3, 0, 0), (2, 3, 1), (3, 0, 1), (2, 2, 0), (4, 0, 0), (4, 0, 1), (3, 3, 0),
-    (3, 3, 1), (4, 3, 1), (4, 3, 0), (3, 2, 0), (3, 2, 1), (4, 2, 1), (4, 2, 0), (3, 1, 0),
-    (3, 1, 1), (5, 4, 1), (5, 4, 0), (4, 1, 0), (5, 5, 1), (4, 1, 1), (5, 3, 0), (5, 3, 1),
-    (5, 5, 0), (6, 4, 1), (5, 6, 1), (5, 6, 0), (6, 4, 0), (5, 1, 0), (5, 2, 1), (5, 2, 0),
-    (6, 5, 1), (6, 3, 0), (5, 1, 1), (6, 5, 0), (6, 3, 1), (5, 7, 0), (5, 0, 0), (5, 0, 1),
-    (6, 6, 1), (6, 6, 0), (7, 0, 0), (5, 7, 1), (7, 0, 1), (6, 2, 0), (6, 2, 1),
+    (1, 7, 1), (1, 1, 1), (1, 1, 0), (0, 0, 0), (1, 7, 0), (8, 0, 1), (1, 2, 1), (1, 2, 0),
+    (2, 0, 1), (8, 0, 0), (1, 6, 0), (2, 0, 0), (2, 7, 1), (1, 6, 1), (2, 7, 0), (1, 4, 1),
+    (1, 4, 0), (2, 1, 0), (2, 2, 1), (2, 1, 1), (2, 2, 0), (2, 6, 0), (2, 4, 1), (2, 5, 1),
+    (2, 3, 1), (2, 4, 0), (2, 5, 0), (2, 6, 1), (3, 0, 0), (2, 3, 0), (3, 1, 0), (3, 1, 1),
+    (4, 1, 1), (4, 1, 0), (3, 3, 0), (3, 3, 1), (4, 3, 1), (4, 3, 0), (3, 2, 0), (3, 2, 1),
+    (4, 2, 0), (3, 0, 1), (5, 4, 0), (5, 4, 1), (4, 0, 0), (4, 2, 1), (5, 3, 1), (5, 5, 0),
+    (5, 5, 1), (5, 2, 1), (5, 3, 0), (4, 0, 1), (5, 6, 0), (5, 2, 0), (5, 7, 0), (6, 4, 1),
+    (5, 6, 1), (6, 4, 0), (5, 7, 1), (6, 5, 0), (5, 1, 1), (6, 3, 1), (6, 3, 0), (6, 5, 1),
+    (5, 1, 0), (6, 2, 1), (5, 0, 0), (7, 0, 0), (6, 6, 0), (5, 0, 1), (7, 0, 1), (6, 6, 1),
+    (6, 2, 0), (6, 7, 0), (6, 7, 1), (6, 1, 1), (6, 1, 0),
 )
 
 
@@ -39,8 +46,7 @@
     tok_hbm, gain_hbm, ids_hbm, log_hbm, wg_hbm, wu_hbm, wd_hbm, out_ref,
     tok, gain, ids, logits, wg, wu, wd,
     lsend, lmeta, msrc, mtab, pbuf, sbuf, xbuf, hid, ysend, r1buf, eacc, pacc, r2send, r2buf, r3send, r3buf,
-    in_sem, w_sem, w_send, w_recv, l_send, l_recv, m_send, m_recv, z_send, z_recv, s2_send, s2_recv,
-    s3_send, x_recv, r1_send, r1_recv, r1_own, r2_send, r2_recv, r3_send, r3_recv,
+    in_sem, w_sem, w_recv, sent, l_recv, m_recv, z_recv, b_recv, s2_recv, x_recv, r1_recv, r2_recv, r3_recv,
 ):
     ep = lax.axis_index("ep")
     c = lax.axis_index("tp")
@@ -94,9 +100,9 @@
 
     for copy in small:
         copy.wait()
-    weights = [pltpu.make_async_copy(src, dst.at[c], w_sem.at[i]) for i, (src, dst) in enumerate(((wg_hbm, wg), (wu_hbm, wu), (wd_hbm, wd)))]
-    for copy in weights:
-        copy.start()
+    weights = ((wg_hbm, wg, 0), (wu_hbm, wu, 0), (wd_hbm, wd, 1))
+    for src, dst, n in weights:
+        pltpu.make_async_copy(src, dst.at[c], w_sem.at[n]).start()
 
     full = tok[...].astype(F32)
     scale = lax.rsqrt(jnp.mean(full * full, axis=-1, keepdims=True) + EPS)
@@ -144,13 +150,13 @@
 
     for col in range(2):
         for j in (1, 3, 2):
-            remote(lsend.at[col, j], lmeta.at[col, (-j) % 4], l_send, l_recv.at[col], peer(col, j))
-            remote(pbuf.at[0, col, 0], pbuf.at[0, col, (-j) % 4], s2_send, s2_recv.at[0, col], peer(col, j))
-    for k in DISTANT:
+            remote(lsend.at[col, j], lmeta.at[col, (-j) % 4], sent, l_recv, peer(col, j))
+            remote(pbuf.at[0, col, 0], pbuf.at[0, col, (-j) % 4], sent, s2_recv.at[0, col], peer(col, j))
+    for k in SINGLE:
         slot = (-k) % NZ
-        remote(pbuf.at[0, :, 0], pbuf.at[slot, :, 0], z_send, z_recv.at[slot], at(dz=k))
-    for i, (src, dst) in enumerate(((wg_hbm, wg), (wu_hbm, wu), (wd_hbm, wd))):
-        remote(src, dst.at[c], w_send, w_recv.at[i], partner)
+        remote(pbuf.at[0, :, 0], pbuf.at[slot, :, 0], sent, z_recv.at[ALONE[slot]], at(dz=k))
+    for src, dst, n in weights:
+        remote(src, dst.at[c], sent, w_recv.at[n], partner)
 
     seen = set()
 
@@ -163,8 +169,8 @@
     def mb(k, col):
         lanes = iota((8, 128), 1) // BLK
         base = jnp.where(iota((8, 128), 0) < 4, lanes * CAP, 0).astype(F32)
+        drain(lsend.at[:, pl.ds(1, 3)], l_recv)
         for col in range(2):
-            drain(lsend.at[col, pl.ds(1, 3)], l_recv.at[col])
             for hi in range(2):
                 t = [lmeta[col, s, hi].astype(F32) for s in range(4)]
                 for lo in range(4):
@@ -175,13 +181,13 @@
                     msrc[hi * 4 + lo, col] = (m + base).astype(BF)
         for k in DISTANT:
             slot = (-k) % NZ
-            remote(msrc.at[k], mtab.at[slot], m_send, m_recv.at[slot], at(dz=k))
+            remote(msrc.at[k], mtab.at[slot], sent, m_recv.at[FAR[slot]], at(dz=k))
 
     def s2(k, col):
         if once(("z", k)):
-            drain(pbuf.at[k, :, 0], z_recv.at[k])
+            drain(pbuf.at[k, :, 0], z_recv.at[ALONE[k]])
         for j in (1, 3, 2):
-            remote(pbuf.at[k, col, 0], pbuf.at[k, col, (-j) % 4], s2_send, s2_recv.at[k, col], peer(col, j))
+            remote(pbuf.at[k, col, 0], pbuf.at[k, col, (-j) % 4], sent, s2_recv.at[ALONE[k], col], peer(col, j))
 
     def table(k, col):
         if k == 0 or k in NEAR:
@@ -197,12 +203,24 @@
             parts.append(jnp.where(sixty == m[j : j + 1, :], value, 0.0).astype(BF))
         return jnp.concatenate(parts, axis=0)
 
+    def lined(k, col):
+        if once(("s2", k, col)):
+            if k in BUNDLE:
+                drain(pbuf.at[k, col], b_recv.at[BUNDLE.index(k), col])
+            else:
+                drain(pbuf.at[k, col, pl.ds(1, 3)], s2_recv.at[ALONE[k], col])
+
+    def zb(k, col):
+        lined(0, col)
+        for k in BUNDLE:
+            slot = (-k) % NZ
+            remote(pbuf.at[0, col], pbuf.at[slot, col], sent, b_recv.at[BUNDLE.index(slot), col], at(dz=k))
+
     def s3(k, col):
         source = 0 if k in NEAR else k
-        if once(("s2", source, col)):
-            drain(pbuf.at[source, col, pl.ds(1, 3)], s2_recv.at[source, col])
+        lined(source, col)
         if k in DISTANT and once(("m", k)):
-            drain(mtab.at[k], m_recv.at[k])
+            drain(mtab.at[k], m_recv.at[FAR[k]])
         rows = pbuf[source, col].reshape(128, HALF)
         packed = jnp.dot(select(k, col, False), rows, preferred_element_type=F32).astype(BF)
         there = (-k) % NZ if k in NEAR else k
@@ -217,7 +235,7 @@
                 sbuf[k, col, j] = pieces[j]
         for j in (1, 3, 2, 0) if k in NEAR else (1, 3, 2):
             device = far(col, j, k if k in NEAR else 0, core)
-            remote(sbuf.at[k, col, j], target((-j) % 4), s3_send.at[1 if k in NEAR else 0], x_recv.at[i, c, col], device)
+            remote(sbuf.at[k, col, j], target((-j) % 4), sent, x_recv.at[i, c], device)
         if k not in NEAR:
 
             @pl.when(c == core)
@@ -230,20 +248,15 @@
             @pl.when(c != core)
             def _():
                 sbuf[k, col, 0] = pieces[0]
-                remote(sbuf.at[k, col, 0], target(0), s3_send.at[2], x_recv.at[i, c, col], partner)
+                remote(sbuf.at[k, col, 0], target(0), sent, x_recv.at[i, c], partner)
 
     def ga(i, h):
         if once(("x", i)):
-            for col in range(2):
-                if PAIRS[i][0] in NEAR:
-                    drain(sbuf.at[0, 0], x_recv.at[i, c, col])
-                else:
-                    drain(sbuf.at[0, 0, pl.ds(1, 3)], x_recv.at[i, c, col])
-                drain(sbuf.at[0, 0], x_recv.at[i, 1 - c, col])
+            drain(sbuf.at[0] if PAIRS[i][0] in NEAR else sbuf.at[0, :, pl.ds(1, 3)], x_recv.at[i, c])
+            drain(sbuf.at[0], x_recv.at[i, 1 - c])
         if once("w"):
-            for n in range(2):
-                weights[n].wait()
-                drain(wg.at[0], w_recv.at[n])
+            drain(wg, w_sem.at[0])
+            drain(wg, w_recv.at[0])
         rows = jnp.concatenate([xbuf[i, s, col].reshape(256, HALF) for s in range(2) for col in range(2)], axis=1)
         gate = jnp.minimum(jnp.dot(rows, wg[h], preferred_element_type=F32), 7.0)
         lin = jnp.clip(jnp.dot(rows, wu[h], preferred_element_type=F32), -7.0, 7.0)
@@ -252,8 +265,8 @@
 
     def db(i, h):
         if once("d"):
-            weights[2].wait()
-            drain(wd.at[0], w_recv.at[2])
+            drain(wd.at[0], w_sem.at[1])
+            drain(wd.at[0], w_recv.at[1])
         hidden = jnp.concatenate([hid[i, 0], hid[i, 1]], axis=1)
         done = jnp.dot(hidden, wd[h], preferred_element_type=F32).astype(BF)
         k0, k1 = PAIRS[i]
@@ -269,7 +282,7 @@
             for j in (1, 3, 2, 0) if close else (1, 3, 2):
                 device = far(col, j, k if close else 0, h)
                 remote(
-                    ysend.at[i, h, col, j], r1buf.at[there, col, (-j) % 4], r1_send.at[1 if close else 0],
+                    ysend.at[i, h, col, j], r1buf.at[there, col, (-j) % 4], sent,
                     r1_recv.at[there, col], device,
                 )
             if not close:
@@ -282,7 +295,7 @@
                 def _():
                     ysend[i, h, col, 0] = pieces[0]
                     remote(
-                        ysend.at[i, h, col, 0], r1buf.at[there, col, 0], r1_send.at[2], r1_own.at[there, col], partner
+                        ysend.at[i, h, col, 0], r1buf.at[there, col, 0], sent, r1_recv.at[there, col], partner
                     )
 
     def to_line(k, col, sums):
@@ -291,19 +304,22 @@
             r2send[k, col, j - 1] = sums[BLK * j : BLK * j + BLK].astype(BF)
         for j in (1, 3, 2):
             remote(
-                r2send.at[k, col, j - 1], r2buf.at[k, col, (-j) % 4 - 1], r2_send.at[1 if k else 0],
-                r2_recv.at[k, col], peer(col, j),
+                r2send.at[k, col, j - 1], r2buf.at[k, col, (-j) % 4 - 1], sent,
+                r2_recv.at[LINED[k], col], peer(col, j),
             )
 
     def u7(k, col):
         if k in NEAR:
             drain(ysend.at[0, 0, 0], r1_recv.at[k, col])
         else:
-            drain(ysend.at[0, 0, 0, pl.ds(1, 3)], r1_recv.at[k, col])
+
+            @pl.when(c == OWNER[k])
+            def _():
+                drain(ysend.at[0, 0, 0, pl.ds(1, 3)], r1_recv.at[k, col])
 
             @pl.when(c != OWNER[k])
             def _():
-                drain(ysend.at[0, 0, 0, 0], r1_own.at[k, col])
+                drain(ysend.at[0, 0, 0], r1_recv.at[k, col])
 
         rows = r1buf[k, col].reshape(256, HALF)
         sums = lax.dot_general(select(k, col, True), rows, (((0,), (0,)), ((), ())), preferred_element_type=F32)
@@ -319,48 +335,44 @@
         to_line(0, col, eacc[col])
 
     def r8(k, col):
-        drain(r2buf.at[k, col], r2_recv.at[k, col])
+        drain(r2buf.at[k, col], r2_recv.at[LINED[k], col])
         total = pacc[k, col]
         for j in range(3):
             total = total + r2buf[k, col, j].astype(F32)
         slot = (-k) % NZ
         r3send[k, col] = total.astype(BF)
-        remote(r3send.at[k, col], r3buf.at[slot, col], r3_send, r3_recv.at[slot, col], at(dz=k))
-
-    steps = (mb, s2, s3, ga, db, u7, r8, e2)
+        remote(r3send.at[k, col], r3buf.at[slot, col], sent, r3_recv, at(dz=k))
+
+    steps = (mb, s2, s3, ga, db, u7, r8, e2, zb)
     for step, k, col in SEQ:
         pl.when(c < 2)(lambda step=step, k=k, col=col: steps[step](k, col))
 
+    part = []
     for col in range(2):
+        drain(r2buf.at[0, col], r2_recv.at[0, col])
         total = pacc[0, col]
-        for k in DISTANT:
-            drain(r3buf.at[k, col], r3_recv.at[k, col])
-            total = total + r3buf[k, col].astype(F32)
-        drain(r2buf.at[0, col], r2_recv.at[0, col])
         for j in range(3):
             total = total + r2buf[0, col, j].astype(F32)
+        part.append(total)
+    drain(r3buf.at[pl.ds(0, NFAR)], r3_recv)
+    for col in range(2):
+        total = part[col]
+        for k in DISTANT:
+            total = total + r3buf[k, col].astype(F32)
         out_ref[:, col * HALF : (col + 1) * HALF] = total.astype(BF)
 
-    six = pl.ds(0, 6)
-    five = pl.ds(0, 5)
-    three = pl.ds(0, 3)
-    rest = pl.ds(1, 3)
-    drain(lsend.at[:, rest], l_send)
-    drain(pbuf.at[five, :, 0], z_send)
-    drain(wg.at[0], w_send)
-    drain(wu.at[0], w_send)
-    drain(wd.at[0], w_send)
-    drain(msrc.at[five], m_send)
-    drain(pbuf.at[six, :, rest], s2_send)
-    drain(sbuf.at[six, :, rest], s3_send.at[0])
-    drain(sbuf.at[pl.ds(0, 2)], s3_send.at[1])
-    drain(sbuf.at[three, :, 0], s3_send.at[2])
-    drain(ysend.at[three, :, :, rest], r1_send.at[0])
-    drain(ysend.at[0], r1_send.at[1])
-    drain(ysend.at[three, 0, :, 0], r1_send.at[2])
-    drain(r2send.at[0], r2_send.at[0])
-    drain(r2send.at[five], r2_send.at[1])
-    drain(r3send.at[five], r3_send)
+    drain(wg, sent)
+    drain(wd.at[0], sent)
+    drain(lsend.at[:, pl.ds(1, 3)], sent)
+    drain(msrc.at[pl.ds(0, NFAR)], sent)
+    drain(pbuf.at[pl.ds(0, len(SINGLE)), :, 0], sent)
+    drain(pbuf.at[pl.ds(0, len(BUNDLE))], sent)
+    drain(pbuf.at[pl.ds(0, len(SINGLE) + 1), :, pl.ds(1, 3)], sent)
+    units = 56 + len(NEAR)
+    for _ in range(2):
+        drain(wg.at[:, pl.ds(0, 16 * units)], sent)
+    drain(r2send.at[pl.ds(0, NFAR + 1)], sent)
+    drain(r3send.at[pl.ds(0, NFAR)], sent)
 
 
 def shards(tokens, norm_gain, routing, route_logits, w_gate, w_up, w_down):
@@ -397,16 +409,18 @@
             vmem((NZ, 2, BLK, HALF), BF),
             vmem((NZ, 2, BLK, HALF), BF),
             dma((4,)),
-            dma((3,)),
-            dma, dma((3,)),
-            dma, dma((2,)),
-            dma, dma((NZ,)),
-            dma, dma((NZ,)),
-            dma, dma((NZ, 2)),
-            dma((3,)), dma((4, 2, 2)),
-            dma((3,)), dma((NZ, 2)), dma((NZ, 2)),
-            dma((2,)), dma((NZ, 2)),
-            dma, dma((NZ, 2)),
+            dma((2,)),
+            dma((2,)),
+            dma,
+            dma,
+            dma((NFAR,)),
+            dma((len(SINGLE) + 1,)),
+            dma((len(BUNDLE), 2)),
+            dma((len(SINGLE) + 1, 2)),
+            dma((4, 2)),
+            dma((NZ, 2)),
+            dma((NFAR + 1, 2)),
+            dma,
         ],
         compiler_params=pltpu.CompilerParams(
             collective_id=0, has_side_effects=True, vmem_limit_bytes=60 * 1024 * 1024

time: 55.3 us -> 52.7 us (0.953)
  Pallas kernels: 54.3 us -> 51.9 us
    pallas_call x1, Pallas kernels: 54.3 us -> 51.9 us  [shards(): pl.pallas_call(kernel, name='routed_layer', out_shape=vmem((BLK, 2 * HALF...]
where the time goes in v5:
time: 52.7 us; the launch traced here: 52.6 us
  Pallas kernels  51.9 us (98%)
  local copies, waits for them, and re-layouts  0.62 us (1%)
    pallas_call x1, Pallas kernels, shards(): pl.pallas_call(kernel, name='routed_layer', out_shape=vmem((BLK, 2 * HALF...  51.9 us

profile of v5, /device:TPU:1, one launch (start us, length us, event | category | flops | bytes accessed | tf_op | source)
XLA Modules:
  0.0 52.6 jit_solution(1585131091046623815)
XLA Ops:
  0.0 51.9 %routed_layer.1 = bf16[32,512]{1,0:T(8,128)(2,1)S(1)} custom-call(bf16[32,1024]{1,0:T(8,128)(2,1)} %tok_hbm.1, f32[1,1024]{1,0:T(1,128)} %bitcast.9, s32[4,32]{1,0:T(4,128)} %bitcast.10, f32[4,32]{1,0:T(4,128)} %bitcast.11, bf16[1024,512]{1,0:T(8,128)(2,1)} %bitcast.6, bf16[1024,512]{1,0:T(8,128)(2,1)} %bitcast.7, bf16[1024,512]{1,0:T(8,128)(2,1)} %bitcast.8), custom_call_target="tpu_custom_call" | custom-call | tf_op jit(solution)/shard_map/routed_layer/pallas_call | solution.py:381
  52.0 0.6 %copy.9 = bf16[32,512]{1,0:T(8,128)(2,1)} copy(bf16[32,512]{1,0:T(8,128)(2,1)S(1)} %routed_layer.1) | data formatting | bytes 65536

commit v6 on v5

--- a/solution.py
+++ b/solution.py
@@ -25,16 +25,16 @@
 OWNER = {k: c for pair in PAIRS for c, k in enumerate(pair)}
 PLACE = {k: i for i, pair in enumerate(PAIRS) for k in pair}
 SEQ = (
-    (1, 7, 1), (1, 1, 1), (1, 1, 0), (0, 0, 0), (1, 7, 0), (8, 0, 1), (1, 2, 1), (1, 2, 0),
-    (2, 0, 1), (8, 0, 0), (1, 6, 0), (2, 0, 0), (2, 7, 1), (1, 6, 1), (2, 7, 0), (1, 4, 1),
-    (1, 4, 0), (2, 1, 0), (2, 2, 1), (2, 1, 1), (2, 2, 0), (2, 6, 0), (2, 4, 1), (2, 5, 1),
-    (2, 3, 1), (2, 4, 0), (2, 5, 0), (2, 6, 1), (3, 0, 0), (2, 3, 0), (3, 1, 0), (3, 1, 1),
-    (4, 1, 1), (4, 1, 0), (3, 3, 0), (3, 3, 1), (4, 3, 1), (4, 3, 0), (3, 2, 0), (3, 2, 1),
-    (4, 2, 0), (3, 0, 1), (5, 4, 0), (5, 4, 1), (4, 0, 0), (4, 2, 1), (5, 3, 1), (5, 5, 0),
-    (5, 5, 1), (5, 2, 1), (5, 3, 0), (4, 0, 1), (5, 6, 0), (5, 2, 0), (5, 7, 0), (6, 4, 1),
-    (5, 6, 1), (6, 4, 0), (5, 7, 1), (6, 5, 0), (5, 1, 1), (6, 3, 1), (6, 3, 0), (6, 5, 1),
-    (5, 1, 0), (6, 2, 1), (5, 0, 0), (7, 0, 0), (6, 6, 0), (5, 0, 1), (7, 0, 1), (6, 6, 1),
-    (6, 2, 0), (6, 7, 0), (6, 7, 1), (6, 1, 1), (6, 1, 0),
+    (1, 1, 1), (1, 1, 0), (0, 0, 0), (8, 0, 1), (1, 7, 1), (1, 7, 0), (1, 6, 1), (2, 0, 1),
+    (1, 2, 1), (1, 6, 0), (2, 0, 0), (1, 2, 0), (2, 7, 0), (2, 7, 1), (1, 4, 1), (2, 1, 0),
+    (1, 4, 0), (8, 0, 0), (2, 6, 0), (2, 1, 1), (2, 2, 0), (2, 2, 1), (2, 6, 1), (2, 5, 1),
+    (2, 4, 1), (2, 4, 0), (3, 0, 0), (2, 5, 0), (2, 3, 1), (2, 3, 0), (3, 0, 1), (3, 1, 0),
+    (4, 0, 0), (3, 1, 1), (4, 1, 1), (4, 1, 0), (3, 3, 0), (3, 3, 1), (4, 3, 0), (3, 2, 0),
+    (3, 2, 1), (4, 2, 0), (4, 3, 1), (4, 2, 1), (5, 4, 0), (5, 2, 1), (5, 5, 1), (5, 5, 0),
+    (5, 3, 0), (5, 6, 0), (5, 4, 1), (5, 3, 1), (4, 0, 1), (5, 2, 0), (6, 4, 0), (6, 2, 1),
+    (5, 6, 1), (6, 5, 0), (5, 1, 0), (5, 7, 1), (5, 7, 0), (5, 1, 1), (6, 5, 1), (6, 4, 1),
+    (6, 3, 0), (5, 0, 0), (7, 0, 0), (6, 6, 0), (6, 3, 1), (6, 6, 1), (6, 2, 0), (5, 0, 1),
+    (7, 0, 1), (6, 7, 1), (6, 1, 0), (6, 7, 0), (6, 1, 1),
 )
 
 
@@ -149,7 +149,7 @@
     pl.semaphore_wait(barrier, len(friends))
 
     for col in range(2):
-        for j in (1, 3, 2):
+        for j in (2, 1, 3):
             remote(lsend.at[col, j], lmeta.at[col, (-j) % 4], sent, l_recv, peer(col, j))
             remote(pbuf.at[0, col, 0], pbuf.at[0, col, (-j) % 4], sent, s2_recv.at[0, col], peer(col, j))
     for k in SINGLE:
@@ -186,7 +186,7 @@
     def s2(k, col):
         if once(("z", k)):
             drain(pbuf.at[k, :, 0], z_recv.at[ALONE[k]])
-        for j in (1, 3, 2):
+        for j in (2, 1, 3):
             remote(pbuf.at[k, col, 0], pbuf.at[k, col, (-j) % 4], sent, s2_recv.at[ALONE[k], col], peer(col, j))
 
     def table(k, col):
@@ -233,7 +233,7 @@
         for j in range(4):
             if j or k in NEAR:
                 sbuf[k, col, j] = pieces[j]
-        for j in (1, 3, 2, 0) if k in NEAR else (1, 3, 2):
+        for j in (1, 3, 2, 0) if k in NEAR else (2, 1, 3):
             device = far(col, j, k if k in NEAR else 0, core)
             remote(sbuf.at[k, col, j], target((-j) % 4), sent, x_recv.at[i, c], device)
         if k not in NEAR:
@@ -279,7 +279,7 @@
             for j in range(4):
                 if j or close:
                     ysend[i, h, col, j] = pieces[j]
-            for j in (1, 3, 2, 0) if close else (1, 3, 2):
+            for j in (1, 3, 2, 0) if close else (2, 1, 3):
                 device = far(col, j, k if close else 0, h)
                 remote(
                     ysend.at[i, h, col, j], r1buf.at[there, col, (-j) % 4], sent,
@@ -302,7 +302,7 @@
         pacc[k, col] = sums[:BLK]
         for j in range(1, 4):
             r2send[k, col, j - 1] = sums[BLK * j : BLK * j + BLK].astype(BF)
-        for j in (1, 3, 2):
+        for j in (2, 1, 3):
             remote(
                 r2send.at[k, col, j - 1], r2buf.at[k, col, (-j) % 4 - 1], sent,
                 r2_recv.at[LINED[k], col], peer(col, j),

time: 52.7 us -> 52.4 us (level)
  no operation moved by 1% of the time
where the time goes in v6:
time: 52.4 us; the launch traced here: 52.3 us
  Pallas kernels  51.6 us (98%)
  local copies, waits for them, and re-layouts  0.62 us (1%)
    pallas_call x1, Pallas kernels, shards(): pl.pallas_call(kernel, name='routed_layer', out_shape=vmem((BLK, 2 * HALF...  51.6 us

profile of v6, /device:TPU:1, one launch (start us, length us, event | category | flops | bytes accessed | tf_op | source)
XLA Modules:
  0.0 52.3 jit_solution(11852915020890575717)
XLA Ops:
  0.0 51.6 %routed_layer.1 = bf16[32,512]{1,0:T(8,128)(2,1)S(1)} custom-call(bf16[32,1024]{1,0:T(8,128)(2,1)} %tok_hbm.1, f32[1,1024]{1,0:T(1,128)} %bitcast.9, s32[4,32]{1,0:T(4,128)} %bitcast.10, f32[4,32]{1,0:T(4,128)} %bitcast.11, bf16[1024,512]{1,0:T(8,128)(2,1)} %bitcast.6, bf16[1024,512]{1,0:T(8,128)(2,1)} %bitcast.7, bf16[1024,512]{1,0:T(8,128)(2,1)} %bitcast.8), custom_call_target="tpu_custom_call" | custom-call | tf_op jit(solution)/shard_map/routed_layer/pallas_call | solution.py:381
  51.6 0.6 %copy.9 = bf16[32,512]{1,0:T(8,128)(2,1)} copy(bf16[32,512]{1,0:T(8,128)(2,1)S(1)} %routed_layer.1) | data formatting | bytes 65536

commit v7 on v6

--- a/solution.py
+++ b/solution.py
@@ -25,16 +25,16 @@
 OWNER = {k: c for pair in PAIRS for c, k in enumerate(pair)}
 PLACE = {k: i for i, pair in enumerate(PAIRS) for k in pair}
 SEQ = (
-    (1, 1, 1), (1, 1, 0), (0, 0, 0), (8, 0, 1), (1, 7, 1), (1, 7, 0), (1, 6, 1), (2, 0, 1),
-    (1, 2, 1), (1, 6, 0), (2, 0, 0), (1, 2, 0), (2, 7, 0), (2, 7, 1), (1, 4, 1), (2, 1, 0),
-    (1, 4, 0), (8, 0, 0), (2, 6, 0), (2, 1, 1), (2, 2, 0), (2, 2, 1), (2, 6, 1), (2, 5, 1),
-    (2, 4, 1), (2, 4, 0), (3, 0, 0), (2, 5, 0), (2, 3, 1), (2, 3, 0), (3, 0, 1), (3, 1, 0),
-    (4, 0, 0), (3, 1, 1), (4, 1, 1), (4, 1, 0), (3, 3, 0), (3, 3, 1), (4, 3, 0), (3, 2, 0),
-    (3, 2, 1), (4, 2, 0), (4, 3, 1), (4, 2, 1), (5, 4, 0), (5, 2, 1), (5, 5, 1), (5, 5, 0),
-    (5, 3, 0), (5, 6, 0), (5, 4, 1), (5, 3, 1), (4, 0, 1), (5, 2, 0), (6, 4, 0), (6, 2, 1),
-    (5, 6, 1), (6, 5, 0), (5, 1, 0), (5, 7, 1), (5, 7, 0), (5, 1, 1), (6, 5, 1), (6, 4, 1),
-    (6, 3, 0), (5, 0, 0), (7, 0, 0), (6, 6, 0), (6, 3, 1), (6, 6, 1), (6, 2, 0), (5, 0, 1),
-    (7, 0, 1), (6, 7, 1), (6, 1, 0), (6, 7, 0), (6, 1, 1),
+    (1, 7, 1), (1, 1, 0), (0, 0, 0), (1, 1, 1), (1, 7, 0), (8, 0, 1), (8, 0, 0), (2, 0, 1),
+    (2, 0, 0), (1, 2, 0), (1, 2, 1), (1, 6, 0), (1, 6, 1), (2, 1, 0), (2, 1, 1), (1, 4, 1),
+    (1, 4, 0), (2, 2, 1), (2, 7, 0), (2, 7, 1), (2, 2, 0), (2, 4, 0), (2, 5, 1), (2, 6, 0),
+    (2, 6, 1), (2, 4, 1), (2, 3, 1), (3, 0, 0), (2, 5, 0), (3, 0, 1), (2, 3, 0), (3, 1, 0),
+    (4, 0, 0), (3, 1, 1), (4, 1, 0), (4, 1, 1), (3, 3, 0), (3, 3, 1), (4, 3, 0), (3, 2, 0),
+    (3, 2, 1), (4, 2, 0), (4, 3, 1), (4, 2, 1), (5, 4, 0), (5, 4, 1), (5, 5, 1), (5, 2, 1),
+    (5, 3, 0), (5, 5, 0), (5, 6, 0), (5, 3, 1), (4, 0, 1), (6, 4, 1), (5, 2, 0), (5, 6, 1),
+    (5, 7, 1), (6, 5, 1), (6, 3, 0), (6, 4, 0), (6, 2, 1), (5, 1, 0), (6, 5, 0), (5, 1, 1),
+    (5, 7, 0), (6, 3, 1), (6, 2, 0), (6, 6, 0), (5, 0, 0), (7, 0, 0), (5, 0, 1), (7, 0, 1),
+    (6, 6, 1), (6, 7, 1), (6, 1, 0), (6, 1, 1), (6, 7, 0),
 )
 
 

time: 52.4 us -> 51.8 us (0.989)
    pallas_call x1, Pallas kernels: 51.6 us -> 51.1 us  [shards(): pl.pallas_call(kernel, name='routed_layer', out_shape=vmem((BLK, 2 * HALF...]
where the time goes in v7:
time: 51.8 us; the launch traced here: 51.7 us
  Pallas kernels  51.1 us (99%)
  local copies, waits for them, and re-layouts  0.62 us (1%)
    pallas_call x1, Pallas kernels, shards(): pl.pallas_call(kernel, name='routed_layer', out_shape=vmem((BLK, 2 * HALF...  51.1 us

profile of v7, /device:TPU:1, one launch (start us, length us, event | category | flops | bytes accessed | tf_op | source)
XLA Modules:
  0.0 51.7 jit_solution(13712983386042205957)
XLA Ops:
  0.0 51.1 %routed_layer.1 = bf16[32,512]{1,0:T(8,128)(2,1)S(1)} custom-call(bf16[32,1024]{1,0:T(8,128)(2,1)} %tok_hbm.1, f32[1,1024]{1,0:T(1,128)} %bitcast.9, s32[4,32]{1,0:T(4,128)} %bitcast.10, f32[4,32]{1,0:T(4,128)} %bitcast.11, bf16[1024,512]{1,0:T(8,128)(2,1)} %bitcast.6, bf16[1024,512]{1,0:T(8,128)(2,1)} %bitcast.7, bf16[1024,512]{1,0:T(8,128)(2,1)} %bitcast.8), custom_call_target="tpu_custom_call" | custom-call | tf_op jit(solution)/shard_map/routed_layer/pallas_call | solution.py:381
  51.1 0.6 %copy.9 = bf16[32,512]{1,0:T(8,128)(2,1)} copy(bf16[32,512]{1,0:T(8,128)(2,1)S(1)} %routed_layer.1) | data formatting | bytes 65536

commit v8 on v7

--- a/solution.py
+++ b/solution.py
@@ -154,7 +154,7 @@
             remote(pbuf.at[0, col, 0], pbuf.at[0, col, (-j) % 4], sent, s2_recv.at[0, col], peer(col, j))
     for k in SINGLE:
         slot = (-k) % NZ
-        remote(pbuf.at[0, :, 0], pbuf.at[slot, :, 0], sent, z_recv.at[ALONE[slot]], at(dz=k))
+        remote(pbuf.at[0, :, 0], pbuf.at[slot, :, 0], sent, z_recv.at[ALONE[slot] - 1], at(dz=k))
     for src, dst, n in weights:
         remote(src, dst.at[c], sent, w_recv.at[n], partner)
 
@@ -185,7 +185,7 @@
 
     def s2(k, col):
         if once(("z", k)):
-            drain(pbuf.at[k, :, 0], z_recv.at[ALONE[k]])
+            drain(pbuf.at[k, :, 0], z_recv.at[ALONE[k] - 1])
         for j in (2, 1, 3):
             remote(pbuf.at[k, col, 0], pbuf.at[k, col, (-j) % 4], sent, s2_recv.at[ALONE[k], col], peer(col, j))
 
@@ -235,7 +235,7 @@
                 sbuf[k, col, j] = pieces[j]
         for j in (1, 3, 2, 0) if k in NEAR else (2, 1, 3):
             device = far(col, j, k if k in NEAR else 0, core)
-            remote(sbuf.at[k, col, j], target((-j) % 4), sent, x_recv.at[i, c], device)
+            remote(sbuf.at[k, col, j], target((-j) % 4), sent, x_recv.at[i], device)
         if k not in NEAR:
 
             @pl.when(c == core)
@@ -248,12 +248,11 @@
             @pl.when(c != core)
             def _():
                 sbuf[k, col, 0] = pieces[0]
-                remote(sbuf.at[k, col, 0], target(0), sent, x_recv.at[i, c], partner)
+                remote(sbuf.at[k, col, 0], target(0), sent, x_recv.at[i], partner)
 
     def ga(i, h):
         if once(("x", i)):
-            drain(sbuf.at[0] if PAIRS[i][0] in NEAR else sbuf.at[0, :, pl.ds(1, 3)], x_recv.at[i, c])
-            drain(sbuf.at[0], x_recv.at[i, 1 - c])
+            drain(wg.at[:, pl.ds(0, 256 if PAIRS[i][0] in NEAR else 224)], x_recv.at[i])
         if once("w"):
             drain(wg, w_sem.at[0])
             drain(wg, w_recv.at[0])
@@ -414,10 +413,10 @@
             dma,
             dma,
             dma((NFAR,)),
-            dma((len(SINGLE) + 1,)),
+            dma((len(SINGLE),)),
             dma((len(BUNDLE), 2)),
             dma((len(SINGLE) + 1, 2)),
-            dma((4, 2)),
+            dma((4,)),
             dma((NZ, 2)),
             dma((NFAR + 1, 2)),
             dma,

time: 51.8 us -> 51.9 us (level)
  no operation moved by 1% of the time
where the time goes in v8:
time: 51.9 us; the launch traced here: 51.8 us
  Pallas kernels  51.1 us (98%)
  local copies, waits for them, and re-layouts  0.62 us (1%)
    pallas_call x1, Pallas kernels, shards(): pl.pallas_call(kernel, name='routed_layer', out_shape=vmem((BLK, 2 * HALF...  51.1 us

profile of v8, /device:TPU:1, one launch (start us, length us, event | category | flops | bytes accessed | tf_op | source)
XLA Modules:
  0.0 51.8 jit_solution(16735791477854764976)
XLA Ops:
  0.0 51.1 %routed_layer.1 = bf16[32,512]{1,0:T(8,128)(2,1)S(1)} custom-call(bf16[32,1024]{1,0:T(8,128)(2,1)} %tok_hbm.1, f32[1,1024]{1,0:T(1,128)} %bitcast.9, s32[4,32]{1,0:T(4,128)} %bitcast.10, f32[4,32]{1,0:T(4,128)} %bitcast.11, bf16[1024,512]{1,0:T(8,128)(2,1)} %bitcast.6, bf16[1024,512]{1,0:T(8,128)(2,1)} %bitcast.7, bf16[1024,512]{1,0:T(8,128)(2,1)} %bitcast.8), custom_call_target="tpu_custom_call" | custom-call | tf_op jit(solution)/shard_map/routed_layer/pallas_call | solution.py:380
  51.2 0.6 %copy.9 = bf16[32,512]{1,0:T(8,128)(2,1)} copy(bf16[32,512]{1,0:T(8,128)(2,1)S(1)} %routed_layer.1) | data formatting | bytes 65536

commit v9 on v8

--- a/solution.py
+++ b/solution.py
@@ -25,15 +25,15 @@
 OWNER = {k: c for pair in PAIRS for c, k in enumerate(pair)}
 PLACE = {k: i for i, pair in enumerate(PAIRS) for k in pair}
 SEQ = (
-    (1, 7, 1), (1, 1, 0), (0, 0, 0), (1, 1, 1), (1, 7, 0), (8, 0, 1), (8, 0, 0), (2, 0, 1),
-    (2, 0, 0), (1, 2, 0), (1, 2, 1), (1, 6, 0), (1, 6, 1), (2, 1, 0), (2, 1, 1), (1, 4, 1),
-    (1, 4, 0), (2, 2, 1), (2, 7, 0), (2, 7, 1), (2, 2, 0), (2, 4, 0), (2, 5, 1), (2, 6, 0),
-    (2, 6, 1), (2, 4, 1), (2, 3, 1), (3, 0, 0), (2, 5, 0), (3, 0, 1), (2, 3, 0), (3, 1, 0),
-    (4, 0, 0), (3, 1, 1), (4, 1, 0), (4, 1, 1), (3, 3, 0), (3, 3, 1), (4, 3, 0), (3, 2, 0),
-    (3, 2, 1), (4, 2, 0), (4, 3, 1), (4, 2, 1), (5, 4, 0), (5, 4, 1), (5, 5, 1), (5, 2, 1),
-    (5, 3, 0), (5, 5, 0), (5, 6, 0), (5, 3, 1), (4, 0, 1), (6, 4, 1), (5, 2, 0), (5, 6, 1),
-    (5, 7, 1), (6, 5, 1), (6, 3, 0), (6, 4, 0), (6, 2, 1), (5, 1, 0), (6, 5, 0), (5, 1, 1),
-    (5, 7, 0), (6, 3, 1), (6, 2, 0), (6, 6, 0), (5, 0, 0), (7, 0, 0), (5, 0, 1), (7, 0, 1),
+    (1, 7, 0), (1, 1, 0), (1, 1, 1), (0, 0, 0), (2, 0, 1), (8, 0, 1), (8, 0, 0), (2, 0, 0),
+    (1, 2, 1), (1, 7, 1), (1, 6, 1), (1, 2, 0), (2, 1, 0), (2, 1, 1), (1, 4, 1), (1, 6, 0),
+    (1, 4, 0), (2, 7, 1), (2, 2, 0), (2, 2, 1), (2, 7, 0), (2, 4, 1), (2, 6, 0), (3, 0, 0),
+    (2, 5, 1), (2, 6, 1), (2, 4, 0), (2, 5, 0), (2, 3, 1), (2, 3, 0), (3, 1, 0), (3, 0, 1),
+    (4, 0, 0), (3, 1, 1), (4, 1, 0), (3, 3, 0), (4, 1, 1), (3, 3, 1), (4, 3, 0), (3, 2, 0),
+    (3, 2, 1), (4, 2, 0), (4, 3, 1), (4, 2, 1), (5, 4, 1), (5, 4, 0), (5, 5, 0), (5, 3, 1),
+    (5, 3, 0), (5, 5, 1), (5, 6, 0), (5, 2, 1), (4, 0, 1), (6, 4, 0), (6, 4, 1), (5, 2, 0),
+    (5, 6, 1), (5, 7, 1), (5, 1, 0), (6, 3, 1), (6, 5, 1), (5, 1, 1), (6, 3, 0), (5, 7, 0),
+    (6, 6, 0), (6, 5, 0), (5, 0, 1), (7, 0, 1), (6, 2, 1), (6, 2, 0), (5, 0, 0), (7, 0, 0),
     (6, 6, 1), (6, 7, 1), (6, 1, 0), (6, 1, 1), (6, 7, 0),
 )
 

time: 51.9 us -> 52.1 us (level)
  no operation moved by 1% of the time
where the time goes in v9:
time: 52.1 us; the launch traced here: 52 us
  Pallas kernels  51.3 us (98%)
  local copies, waits for them, and re-layouts  0.62 us (1%)
    pallas_call x1, Pallas kernels, shards(): pl.pallas_call(kernel, name='routed_layer', out_shape=vmem((BLK, 2 * HALF...  51.3 us

profile of v9, /device:TPU:1, one launch (start us, length us, event | category | flops | bytes accessed | tf_op | source)
XLA Modules:
  0.0 52.0 jit_solution(12984138439938863167)
XLA Ops:
  0.0 51.3 %routed_layer.1 = bf16[32,512]{1,0:T(8,128)(2,1)S(1)} custom-call(bf16[32,1024]{1,0:T(8,128)(2,1)} %tok_hbm.1, f32[1,1024]{1,0:T(1,128)} %bitcast.9, s32[4,32]{1,0:T(4,128)} %bitcast.10, f32[4,32]{1,0:T(4,128)} %bitcast.11, bf16[1024,512]{1,0:T(8,128)(2,1)} %bitcast.6, bf16[1024,512]{1,0:T(8,128)(2,1)} %bitcast.7, bf16[1024,512]{1,0:T(8,128)(2,1)} %bitcast.8), custom_call_target="tpu_custom_call" | custom-call | tf_op jit(solution)/shard_map/routed_layer/pallas_call | solution.py:380
  51.3 0.6 %copy.9 = bf16[32,512]{1,0:T(8,128)(2,1)} copy(bf16[32,512]{1,0:T(8,128)(2,1)S(1)} %routed_layer.1) | data formatting | bytes 65536

commit v10 on v7

--- a/solution.py
+++ b/solution.py
@@ -150,8 +150,8 @@
 
     for col in range(2):
         for j in (2, 1, 3):
+            remote(pbuf.at[0, col, 0], pbuf.at[0, col, (-j) % 4], sent, s2_recv.at[0, col], peer(col, j))
             remote(lsend.at[col, j], lmeta.at[col, (-j) % 4], sent, l_recv, peer(col, j))
-            remote(pbuf.at[0, col, 0], pbuf.at[0, col, (-j) % 4], sent, s2_recv.at[0, col], peer(col, j))
     for k in SINGLE:
         slot = (-k) % NZ
         remote(pbuf.at[0, :, 0], pbuf.at[slot, :, 0], sent, z_recv.at[ALONE[slot]], at(dz=k))

time: 51.8 us -> 51.8 us (level)
  no operation moved by 1% of the time
where the time goes in v10:
time: 51.8 us; the launch traced here: 51.7 us
  Pallas kernels  51 us (98%)
  local copies, waits for them, and re-layouts  0.62 us (1%)
    pallas_call x1, Pallas kernels, shards(): pl.pallas_call(kernel, name='routed_layer', out_shape=vmem((BLK, 2 * HALF...  51 us

profile of v10, /device:TPU:1, one launch (start us, length us, event | category | flops | bytes accessed | tf_op | source)
XLA Modules:
  0.0 51.7 jit_solution(10354928515680141885)
XLA Ops:
  0.0 51.0 %routed_layer.1 = bf16[32,512]{1,0:T(8,128)(2,1)S(1)} custom-call(bf16[32,1024]{1,0:T(8,128)(2,1)} %tok_hbm.1, f32[1,1024]{1,0:T(1,128)} %bitcast.9, s32[4,32]{1,0:T(4,128)} %bitcast.10, f32[4,32]{1,0:T(4,128)} %bitcast.11, bf16[1024,512]{1,0:T(8,128)(2,1)} %bitcast.6, bf16[1024,512]{1,0:T(8,128)(2,1)} %bitcast.7, bf16[1024,512]{1,0:T(8,128)(2,1)} %bitcast.8), custom_call_target="tpu_custom_call" | custom-call | tf_op jit(solution)/shard_map/routed_layer/pallas_call | solution.py:381
  51.0 0.6 %copy.9 = bf16[32,512]{1,0:T(8,128)(2,1)} copy(bf16[32,512]{1,0:T(8,128)(2,1)S(1)} %routed_layer.1) | data formatting | bytes 65536
